TPU v7x, 256 devices: a whole 4x4x8 slice. The times are simulated.
256 devices in a mesh: ep: 64 (over z, x, core), tp: 4 (over y).
Axes of the slice: x: 4, y: 4, z: 8, core: 2. Of those that a mesh axis runs over, the one named last changes fastest.
Arguments:
- queries: bfloat16 [16384, 8, 128], P('ep', 'tp'), may hold values from -256 to 256
- keys: bfloat16 [16384, 4, 128], P('ep', 'tp'), may hold values from -8 to 8
- values: bfloat16 [16384, 4, 128], P('ep', 'tp'), may hold values from -6 to 6
- attn_lambda: float32 [8], P('tp'), may hold values from 0.3 to 0.8
- head_gain: float32 [128], replicated, may hold values from 0.1 to 1.9
- w_out: bfloat16 [1024, 2048], replicated, may hold values from -0.1875 to 0.1875
- moe_rows: bfloat16 [32768, 2048], P('ep'), may hold values from -6 to 6
- moe_gain: float32 [2048], replicated, may hold values from 0.1 to 1.9
- routes: int32 [32768, 2], P('ep'), may hold values from 0 to 63, all different within a row; in each aligned block of 128 rows (0 to 127, 128 to 255, ...) at most 8 rows name the same one
- route_weights: float32 [32768, 2], P('ep'), may hold values from 0.1 to 1
- w_gate: bfloat16 [64, 2048, 1024], P('ep', None, 'tp'), may hold values from -0.125 to 0.125
- w_up: bfloat16 [64, 2048, 1024], P('ep', None, 'tp'), may hold values from -0.125 to 0.125
- w_down: bfloat16 [64, 1024, 2048], P('ep', 'tp'), may hold values from -0.1875 to 0.1875
Outputs:
- mixer_out: bfloat16 [16384, 2048], P(('ep', 'tp'))
- moe_out: bfloat16 [32768, 2048], P(('ep', 'tp'))
Inputs may be any that keep to these rules, and one draw needn't show every extreme that they name: `routes`: each row names 2 different experts. In each aligned block of 128 rows (the rows of moe_out that one device holds) no expert is named by more than 8 rows, a bound that some block reaches.
All inputs are finite; a program needn't handle non-finite values.
Results may differ from a plain program's by a relative error of at most 0.011.
Values may be sent and summed in bfloat16 or wider, within the bound.
No kernel may reach another device: no remote copies, remote signals or barrier semaphores. Data moves between devices by JAX's collectives and lax.ppermute only.
A program may use at most 128 MiB of HBM per device.

v0:
```python
import jax
import jax.numpy as jnp
from jax import lax
from jax.sharding import PartitionSpec as P

EPSILON = 1e-06
MASKED = -1e30


def split_up(x, dim, size):
    before, after = (x.shape[:dim], x.shape[dim + 1 :])
    return jnp.moveaxis(x.reshape(*before, size, -1, *after), dim, 0)


def sum_at_owner(x, axis, dim):
    size = lax.axis_size(axis)
    tiles = lax.all_to_all(split_up(x, dim, size), axis, 0, 0, tiled=True)
    return jnp.sum(tiles.astype(jnp.float32), axis=0)


def joined_along(tiles, dim):
    tiles = jnp.moveaxis(tiles, 0, dim)
    lengths = tiles.shape
    return tiles.reshape(*lengths[:dim], lengths[dim] * lengths[dim + 1], *lengths[dim + 2 :])


def piecewise(x, axis, dim, work, out_dim):
    span = x.shape[dim]
    pieces = jnp.split(x, 2, axis=dim) if span % 2 == 0 else [x]
    first = jnp.arange(lax.axis_size(axis)) * span
    tiles = [lax.all_gather(section, axis) for section in pieces]
    made = [jax.vmap(work)(b, first + k * (span // len(pieces))) for k, b in enumerate(tiles)]
    return joined_along(jnp.concatenate(made, axis=out_dim + 1), out_dim)


def rms_scaled(values_f, gain):
    mean_sq = jnp.mean(values_f * values_f, axis=-1, keepdims=True)
    return values_f * lax.rsqrt(mean_sq + EPSILON) * gain


def slot_numbers(block_routes, experts):
    flat_ids = block_routes.reshape(-1)
    matches = (flat_ids[:, None] == lax.iota(jnp.int32, experts)[None, :]).astype(jnp.int32)
    earlier = jnp.cumsum(matches, axis=0) - matches
    return jnp.sum(earlier * matches, axis=1).reshape(block_routes.shape)


def fill_slots(block_rows, block_routes, experts, capacity):
    slot_ids = slot_numbers(block_routes, experts)
    model_width = block_rows.shape[1]
    copies = jnp.broadcast_to(block_rows[:, None, :], block_routes.shape + (model_width,))
    blank_slots = jnp.zeros((experts, capacity, model_width), block_rows.dtype)
    return (blank_slots.at[block_routes, slot_ids].set(copies), slot_ids)


def local(
    queries,
    keys,
    values,
    attn_lambda,
    head_gain,
    w_out,
    moe_rows,
    moe_gain,
    routes,
    route_weights,
    w_gate,
    w_up,
    w_down,
):
    positions = queries.shape[0]
    q_heads = queries.shape[1]
    kv_heads = keys.shape[1]
    head_dim = queries.shape[2] // 2
    value_dim = values.shape[2]
    per_key = q_heads // kv_heads
    first_pos = lax.axis_index("ep") * positions
    query_pos = first_pos + lax.iota(jnp.int32, positions)
    last_pos = first_pos + positions - 1
    query_view = queries.reshape(positions, kv_heads, per_key, 2, head_dim)
    inv_scale = head_dim ** (-0.5)
    start_max = jnp.full((positions, kv_heads, per_key, 2), MASKED, jnp.float32)
    start_total = jnp.zeros((positions, kv_heads, per_key, 2), jnp.float32)
    start_acc = jnp.zeros((positions, kv_heads, per_key, 2, value_dim), jnp.float32)
    carry = (start_max, start_total, start_acc)
    key_piece = lax.all_gather(keys, "ep", axis=0, tiled=True)
    value_piece = lax.all_gather(values, "ep", axis=0, tiled=True)
    shard_count = key_piece.shape[0] // positions
    together = 1
    for candidate in (2, 3, 4):
        if shard_count % candidate == 0:
            together = candidate
    block_len = together * positions
    blocks = shard_count // together
    key_blocks = key_piece.reshape(blocks, block_len, kv_heads, 2, head_dim)
    value_blocks = value_piece.reshape(blocks, block_len, kv_heads, value_dim)
    block_starts = block_len * lax.iota(jnp.int32, blocks)

    def visit(running, inputs):
        key_blk, value_blk, block_start = inputs

        def update(current):
            run_max, run_total, run_acc = current
            key_pos = block_start + lax.iota(jnp.int32, block_len)
            scores = (
                jnp.einsum(
                    "qkgmd,pkmd->qkgmp", query_view, key_blk, preferred_element_type=jnp.float32
                )
                * inv_scale
            )
            allowed = key_pos[None, :] <= query_pos[:, None]
            scores = jnp.where(allowed[:, None, None, None, :], scores, MASKED)
            new_max = jnp.maximum(run_max, jnp.max(scores, axis=-1))
            shrink = jnp.exp(run_max - new_max)
            weights = jnp.exp(scores - new_max[..., None])
            run_total = run_total * shrink + jnp.sum(weights, axis=-1)
            run_acc = run_acc * shrink[..., None] + jnp.einsum(
                "qkgmp,pkv->qkgmv",
                weights.astype(jnp.bfloat16),
                value_blk,
                preferred_element_type=jnp.float32,
            )
            return (new_max, run_total, run_acc)

        def keep(current):
            return current

        return (lax.cond(block_start <= last_pos, update, keep, running), None)

    carry, unused = lax.scan(visit, carry, (key_blocks, value_blocks, block_starts))
    run_max, run_total, run_acc = carry
    ratios = run_acc / run_total[..., None]
    lambda_view = attn_lambda.reshape(1, kv_heads, per_key, 1)
    head_out = ratios[:, :, :, 0] - lambda_view * ratios[:, :, :, 1]
    attn_rows = (
        rms_scaled(head_out, head_gain).astype(jnp.bfloat16).reshape(positions, q_heads * value_dim)
    )
    tp_count = lax.axis_size("tp")
    tp_id = lax.axis_index("tp")
    head_width = q_heads * value_dim
    w_local = lax.dynamic_slice_in_dim(w_out, tp_id * head_width, head_width, 0)
    mixer_out = sum_at_owner(
        jnp.dot(attn_rows, w_local, preferred_element_type=jnp.float32).astype(jnp.bfloat16),
        "tp",
        0,
    ).astype(jnp.bfloat16)
    experts = lax.axis_size("ep")
    dev_rows = moe_rows.shape[0] // tp_count
    top_count = routes.shape[1]
    capacity = max(2, 2 * dev_rows * top_count // experts)
    model_width = moe_rows.shape[1]
    hidden_units = w_gate.shape[2]
    own_routes = lax.dynamic_slice_in_dim(routes, tp_id * dev_rows, dev_rows, 0)
    own_weights = lax.dynamic_slice_in_dim(route_weights, tp_id * dev_rows, dev_rows, 0)

    def expert_hidden(slot_rows):
        flat_rows = slot_rows.reshape(-1, model_width)
        gate_out = jnp.dot(flat_rows, w_gate[0], preferred_element_type=jnp.float32)
        up_out = jnp.dot(flat_rows, w_up[0], preferred_element_type=jnp.float32)
        return (
            (jax.nn.silu(gate_out) * up_out)
            .astype(jnp.bfloat16)
            .reshape(slot_rows.shape[:-1] + (hidden_units,))
        )

    own_rows = rms_scaled(
        lax.dynamic_slice_in_dim(moe_rows, tp_id * dev_rows, dev_rows, 0).astype(jnp.float32),
        moe_gain,
    ).astype(jnp.bfloat16)
    outgoing, own_slots = fill_slots(own_rows, own_routes, experts, capacity)
    arrived = lax.all_to_all(outgoing, "ep", split_axis=0, concat_axis=0, tiled=True)

    def hidden_piece(slot_rows, begin_row):
        return expert_hidden(slot_rows)

    hidden = piecewise(arrived[None], "tp", 0, hidden_piece, 0)
    all_units = lax.all_to_all(hidden, "tp", split_axis=0, concat_axis=3, tiled=True)
    down_whole = lax.all_gather(w_down[0], "tp", axis=0, tiled=True)
    flat_units = all_units.reshape(-1, tp_count * hidden_units)
    summed_f = jnp.zeros((flat_units.shape[0], model_width), jnp.float32)
    for group in range(tp_count):
        unit_block = flat_units[:, group * hidden_units : (group + 1) * hidden_units]
        weight_block = down_whole[group * hidden_units : (group + 1) * hidden_units]
        group_part = jnp.dot(unit_block, weight_block, preferred_element_type=jnp.float32).astype(
            jnp.bfloat16
        )
        summed_f = summed_f + group_part.astype(jnp.float32)
    summed = summed_f.astype(jnp.bfloat16).reshape(all_units.shape[:-1] + (model_width,))
    returned = lax.all_to_all(summed, "ep", split_axis=1, concat_axis=1, tiled=True)[0]
    picked = returned[own_routes, own_slots]
    moe_out = jnp.sum(own_weights[..., None] * picked.astype(jnp.float32), axis=1).astype(
        jnp.bfloat16
    )
    return (mixer_out, moe_out)


def solution(mesh):
    return jax.shard_map(
        local,
        mesh=mesh,
        in_specs=(
            P("ep", "tp", None),
            P("ep", "tp", None),
            P("ep", "tp", None),
            P("tp"),
            P(),
            P(),
            P("ep", None),
            P(),
            P("ep", None),
            P("ep", None),
            P("ep", None, "tp"),
            P("ep", None, "tp"),
            P("ep", "tp", None),
        ),
        out_specs=(P(("ep", "tp"), None), P(("ep", "tp"), None)),
        check_vma=False,
    )
```

profile of v0, /device:TPU:2, one launch (start us, length us, event | category | flops | bytes accessed | tf_op | source)
XLA Modules:
  0.0 434.8 jit_solution(10305571413842020620)
XLA Ops:
  7.2 0.7 all-gather.7.cloned.1.call-update
  8.0 0.7 all-gather.9.cloned.1.call-update
  8.7 0.7 constant_dynamic-slice_fusion
  9.8 0.6 reduce-window.6
  10.4 0.2 slice_reduce_fusion
  10.8 0.1 reshape.234
  11.1 1.2 fusion.25
  12.3 1.3 fusion.27
  13.6 0.6 broadcast_in_dim.57
  14.2 1.2 reshape.247
  15.5 0.2 broadcast_in_dim.36
  15.7 33.0 %scatter_fusion = bf16[64,8,2048]{2,1,0:T(8,128)(2,1)S(1)} fusion(bf16[64,8,2048]{2,1,0:T(8,128)(2,1)S(1)} %broadcast_in_dim.36, s32[256]{0:T(256)S(1)} %reshape.245, bf16[256,2048]{1,0:T(8,128)(2,1)} %reshape.247), kind=kCustom, calls=%fused_computation.1 | custom fusion | bytes 3147776 | tf_op jit(solution)/shard_map/scatter | solution.py:53
  48.8 73.1 %all_to_all.30 = bf16[64,8,2048]{2,1,0:T(8,128)(2,1)} all-to-all(bf16[64,8,2048]{2,1,0:T(8,128)(2,1)S(1)} %scatter_fusion), channel_id=1, replica_groups=mesh['ep'=64,'tp'=4] {'ep'}, dimensions={0} | all-to-all | bytes 4194304 | tf_op jit(solution)/shard_map/all_to_all | solution.py:171
  121.9 0.2 all-gather.13.cloned.1.call-start
  122.1 0.3 all-gather.13.cloned.1.call-update
  122.7 14.7 %reshape.263 = bf16[16,1024,1,2,64]{4,3,1,0,2:T(2,128)(2,1)} reshape(bf16[16384,1,128]{2,0,1:T(8,128)(2,1)} %all-gather.7.cloned.1.call-done) | data formatting | bytes 8388608 | tf_op jit(solution)/shard_map/reshape | solution.py:95
  137.4 20.2 %copy.37 = bf16[16,1024,1,2,64]{1,4,3,2,0:T(8,128)(2,1)} copy(bf16[16,1024,1,2,64]{4,3,1,0,2:T(2,128)(2,1)} %reshape.263) | data formatting | bytes 8388608
  157.6 29.6 %all-gather.9.cloned.1.call-done = bf16[16384,1,128]{2,0,1:T(8,128)(2,1)} async-done(((bf16[256,1,128]{2,0,1:T(8,128)(2,1)}), bf16[16384,1,128]{2,0,1:T(8,128)(2,1)}) %all-gather.9.cloned.1.call-update) | async-done | bytes 4194320 | tf_op jit(solution)/shard_map/all_gather | solution.py:87
  187.2 6.4 %copy.39 = bf16[16,1024,1,128]{1,3,2,0:T(8,128)(2,1)} copy(bf16[16,1024,1,128]{3,1,0,2:T(8,128)(2,1)} %bitcast.160) | data formatting | bytes 8388608
  193.6 23.8 %while.15 = (s32[]{:T(128)}, f32[256,1,2,2]{0,2,3,1:T(2,128)S(1)}, f32[256,1,2,2]{0,2,3,1:T(2,128)S(1)}, f32[256,1,2,2,128]{0,4,3,2,1:T(8,128)S(1)}, s32[16]{0:T...) while((s32[]{:T(128)}, f32[256,1,2,2]{0,2,3,1:T(2,128)S(1)}, ...), condition=%wide.region_5.6_spmd.clone, body=%wide.region_0.5_spmd.clone.sunk | while | flops 411570432 | bytes 15156511 | solution.py:130
  193.6 0.6 dynamic_slice.56
  194.8 5.2 %conditional.3 = ((f32[256,1,2,2]{0,2,3,1:T(2,128)S(1)}, f32[256,1,2,2]{0,2,3,1:T(2,128)S(1)}, f32[256,1,2,2,128]{0,4,3,2,1:T(8,128)S(1)})) conditional(s32[]{:T(128)} %convert_element_type.131, (f32[256,1,2,2]{0,2,3,1:T(2,128)S(1)}, f32[256,1,2,2]{0,2,3,1:T(2,128)S(1)}, f32[256,1,2,2,128]{0,4,3,2,1:T(8,128)S(1)}) %tuple.48, (s32[]{:T(128)}, ...), branch_computations={%region_1.1_spmd, %region_2.4_spmd} | conditional | flops 411570432 | bytes 15155240 | solution.py:128
  194.8 0.5 iota_add_fusion
  195.4 0.2 broadcast_compare_fusion
  195.6 1.8 fusion.4
  197.4 1.0 fusion.5
  198.4 1.5 fusion.11
  200.0 0.6 dynamic_slice.56
  201.2 0.6 dynamic_slice.56
  202.3 0.6 dynamic_slice.56
  203.5 0.6 dynamic_slice.56
  204.7 0.6 dynamic_slice.56
  205.8 0.6 dynamic_slice.56
  207.0 0.6 dynamic_slice.56
  208.1 0.6 dynamic_slice.56
  209.3 0.6 dynamic_slice.56
  210.5 0.6 dynamic_slice.56
  211.6 0.6 dynamic_slice.56
  212.8 0.6 dynamic_slice.56
  214.0 0.6 dynamic_slice.56
  215.1 0.6 dynamic_slice.56
  216.3 0.6 dynamic_slice.56
  217.5 55.6 %all-gather.11.cloned.1.call-done = bf16[256,8,2048]{2,1,0:T(8,128)(2,1)} async-done(((bf16[64,8,2048]{2,1,0:T(8,128)(2,1)}), bf16[256,8,2048]{2,1,0:T(8,128)(2,1)}) %all-gather.11.cloned.1.call-update) | async-done | bytes 8388624 | tf_op jit(solution)/shard_map/all_gather | solution.py:31
  273.1 5.9 %fusion.28 = f32[4,512,256]{2,1,0:T(8,128)S(1)} fusion(bf16[4,512,2048]{2,1,0:T(8,128)(2,1)} %bitcast.170, bf16[1,2048,256]{2,1,0:T(8,128)(2,1)S(1)} %copy-done), kind=kOutput, calls=%fused_computation.47 | convolution fusion | flops 2147483648 | bytes 11534336 | tf_op jit(solution)/shard_map/vmap()/dot_general | solution.py:159
  279.1 3.6 fusion.24
  282.7 4.0 all-to-all-start.2
  287.0 2.8 convolution_convert_fusion.4
  289.8 22.2 %all-to-all-done.2 = bf16[4,64,8,256]{3,2,1,0:T(8,128)(2,1)S(1)} async-done(((bf16[4,64,8,256]{3,2,1,0:T(8,128)(2,1)}), bf16[4,64,8,256]{3,2,1,0:T(8,128)(2,1)S(1)}, u32[]{:S(2)}, u32[]{:S(2)}) %all-to-all-start.2) | async-done | bytes 1048608 | tf_op jit(solution)/shard_map/all_to_all | solution.py:177
  312.0 3.7 all-to-all-start
  315.7 1.4 copy.65
  317.1 0.2 copy.56
  317.3 29.3 %all-gather.13.cloned.1.call-done = bf16[1,1024,2048]{2,1,0:T(8,128)(2,1)} async-done(((bf16[1,256,2048]{2,1,0:T(8,128)(2,1)}), bf16[1,1024,2048]{2,1,0:T(8,128)(2,1)}) %all-gather.13.cloned.1.call-update) | async-done | bytes 4194320 | tf_op jit(solution)/shard_map/all_gather | solution.py:178
  346.6 2.1 convolution_convert_fusion
  348.7 1.9 convolution_convert_fusion.1
  350.7 0.7 convolution_convert_fusion.2
  351.4 2.6 fusion.23
  354.0 1.0 copy-done.2
  355.0 10.6 %all-to-all-start.3 = ((bf16[1,64,8,2048]{3,2,0,1:T(8,128)(2,1)}), bf16[1,64,8,2048]{3,2,0,1:T(8,128)(2,1)S(1)}, u32[]{:S(2)}, u32[]{:S(2)}) async-start(bf16[1,64,8,2048]{3,2,0,1:T(8,128)(2,1)} %fusion.23), calls=%async_computation.3 | async-start | bytes 4194304 | tf_op jit(solution)/shard_map/all_to_all | solution.py:189
  365.7 0.7 constant_dynamic-slice_fusion.1
  366.5 2.2 reduce_sum.60
  368.7 48.1 %all-to-all-done.3 = bf16[1,64,8,2048]{3,2,0,1:T(8,128)(2,1)S(1)} async-done(((bf16[1,64,8,2048]{3,2,0,1:T(8,128)(2,1)}), bf16[1,64,8,2048]{3,2,0,1:T(8,128)(2,1)S(1)}, u32[]{:S(2)}, u32[]{:S(2)}) %all-to-all-start.3) | async-done | bytes 2097184 | tf_op jit(solution)/shard_map/all_to_all | solution.py:189
  416.8 5.2 %gather_fusion = bf16[256,2048]{1,0:T(8,128)(2,1)} fusion(bf16[64,8,2048]{2,1,0:T(8,128)(2,1)S(1)} %bitcast.159, s32[256]{0:T(256)S(1)} %reshape.239), kind=kCustom, calls=%fused_computation | custom fusion | bytes 2099200 | tf_op jit(solution)/shard_map/gather | solution.py:190
  422.0 2.4 reshape.258
  424.4 3.9 multiply_reduce_fusion
  (82 shorter events, 2.2 us)
Async XLA Ops:
  7.2 266.0 %copy-start = (bf16[1,2048,256]{2,1,0:T(8,128)(2,1)S(1)}, bf16[1,2048,256]{2,1,0:T(8,128)(2,1)}, u32[]{:S(2)}) copy-start(bf16[1,2048,256]{2,1,0:T(8,128)(2,1)} %param.28) | copy-start | bytes 3145732
  7.2 115.6 %all-gather.7.cloned.1.call-start = ((), (), s32[]{:S(2)}) async-start(), calls=%async_computation.4 | async-start | bytes 4259840 | tf_op jit(solution)/shard_map/all_gather | solution.py:86
  7.9 179.3 %all-gather.9.cloned.1.call-start = ((), (), s32[]{:S(2)}) async-start(), calls=%async_computation.5 | async-start | bytes 4259840 | tf_op jit(solution)/shard_map/all_gather | solution.py:87
  8.7 264.5 %all-gather.11.cloned.1.call-start = ((), (), s32[]{:S(2)}) async-start(), calls=%async_computation.6 | async-start | bytes 10485760 | tf_op jit(solution)/shard_map/all_gather | solution.py:31
  48.7 73.8 %copy-start.3 = (bf16[256,2,128]{2,1,0:T(2,128)(2,1)S(1)}, bf16[256,2,128]{2,1,0:T(2,128)(2,1)}, u32[]{:S(2)}) copy-start(bf16[256,2,128]{2,1,0:T(2,128)(2,1)} %param.17) | copy-start | bytes 393220
  48.7 73.9 %copy-start.4 = (f32[2]{0:T(128)S(1)}, f32[2]{0:T(128)}, u32[]{:S(2)}) copy-start(f32[2]{0:T(128)} %param.20) | copy-start | bytes 28
  48.7 73.9 %copy-start.5 = (f32[128]{0:T(128)S(1)}, f32[128]{0:T(128)}, u32[]{:S(2)}) copy-start(f32[128]{0:T(128)} %param.21) | copy-start | bytes 1540
  121.9 224.7 %all-gather.13.cloned.1.call-start = ((), (), s32[]{:S(2)}) async-start(), calls=%async_computation.7 | async-start | bytes 5242880 | tf_op jit(solution)/shard_map/all_gather | solution.py:178
  273.1 5.9 %copy-start.6 = (bf16[256,8,2048]{2,1,0:T(8,128)(2,1)S(1)}, bf16[256,8,2048]{2,1,0:T(8,128)(2,1)}, u32[]{:S(2)}) copy-start(bf16[256,8,2048]{2,1,0:T(8,128)(2,1)} %all-gather.11.cloned.1.call-done) | copy-start | bytes 25165828
  273.1 6.0 %copy-start.7 = (bf16[1,2048,256]{2,1,0:T(8,128)(2,1)S(1)}, bf16[1,2048,256]{2,1,0:T(8,128)(2,1)}, u32[]{:S(2)}) copy-start(bf16[1,2048,256]{2,1,0:T(8,128)(2,1)} %param.27) | copy-start | bytes 3145732
  282.7 29.3 %all-to-all-start.2 = ((bf16[4,64,8,256]{3,2,1,0:T(8,128)(2,1)}), bf16[4,64,8,256]{3,2,1,0:T(8,128)(2,1)S(1)}, u32[]{:S(2)}, u32[]{:S(2)}) async-start(bf16[4,64,8,256]{3,2,1,0:T(8,128)(2,1)} %fusion.24), calls=%async_computation.2 | async-start | bytes 2097152 | tf_op jit(solution)/shard_map/all_to_all | solution.py:177
  312.0 42.0 %all-to-all-start = ((bf16[4,64,2048]{2,1,0:T(8,128)(2,1)}), bf16[4,64,2048]{2,1,0:T(8,128)(2,1)S(1)}, u32[]{:S(2)}, u32[]{:S(2)}) async-start(bf16[4,64,2048]{2,1,0:T(8,128)(2,1)} %bitcast.26), calls=%async_computation | async-start | bytes 2097152 | tf_op jit(solution)/shard_map/all_to_all | solution.py:17
  346.6 4.0 copy-start.1
  354.0 1.0 copy-start.2
  355.0 61.8 %all-to-all-start.3 = ((bf16[1,64,8,2048]{3,2,0,1:T(8,128)(2,1)}), bf16[1,64,8,2048]{3,2,0,1:T(8,128)(2,1)S(1)}, u32[]{:S(2)}, u32[]{:S(2)}) async-start(bf16[1,64,8,2048]{3,2,0,1:T(8,128)(2,1)} %fusion.23), calls=%async_computation.3 | async-start | bytes 4194304 | tf_op jit(solution)/shard_map/all_to_all | solution.py:189
Sparse Core Ops, SparseCore 0:
  10.8 94.4 all-gather.6
  108.0 79.1 all-gather.8
  189.0 84.0 all-gather.10
  274.8 71.7 all-gather.12
where the time goes:
time: 438 us; the launch traced here: 435 us
  waiting for transfers between devices  187 us (43%)
  local copies, waits for them, and re-layouts  98.3 us (22%)
  blocking collectives  73.1 us (17%)
  matrix products  22.9 us (5%)
  starting transfers between devices  18.6 us (4%)
  between operations  14.1 us (3%)
  other arithmetic  11.5 us (3%)
  loops' own time  9.72 us (2%)
    all_to_all x1, blocking collectives, local(): lax.all_to_all(outgoing, 'ep', split_axis=0, concat_axis=0, tiled=True)  73.1 us
    all_gather x1, waiting for transfers between devices, piecewise(): tiles = [lax.all_gather(section, axis) for section in pieces]  55.6 us
    all_to_all x1, waiting for transfers between devices, local(): lax.all_to_all(summed, 'ep', split_axis=1, concat_axis=1, tiled=True)[0]  48.1 us
    scatter x1, local copies, waits for them, and re-layouts, fill_slots(): return (blank_slots.at[block_routes, slot_ids].set(copies), slot_ids)  33 us
    all_gather x1, waiting for transfers between devices, local(): value_piece = lax.all_gather(values, 'ep', axis=0, tiled=True)  29.6 us
    all_gather x1, waiting for transfers between devices, local(): down_whole = lax.all_gather(w_down[0], 'tp', axis=0, tiled=True)  29.3 us
    unnamed x22, local copies, waits for them, and re-layouts  28.1 us
    all_to_all x1, waiting for transfers between devices, local(): lax.all_to_all(hidden, 'tp', split_axis=0, concat_axis=3, tiled=True)  22.2 us
  transfers between devices with their start and end apart: 7, of which 5 were waited for; matrix products, arithmetic and copies ran while one was open for 28% of the time, Pallas kernels for 0%

commit v1 on v0

v1 whole, which is shorter than its diff:
```python
import functools

import jax
import jax.numpy as jnp
from jax import lax
from jax.experimental import pallas as pl
from jax.experimental.pallas import tpu as pltpu
from jax.sharding import PartitionSpec as P


EPSILON = 1e-06
MASKED = -1e30
KEY_BLOCK = 1024


def attention_body(place_ref, lam_ref, q_ref, kv_ref, gain_ref, out_ref, qs_ref, max_ref, acc_ref, *, heads, dim):
    rows = q_ref.shape[0]
    width = 2 * dim
    first = place_ref[0] * rows
    lane = lax.broadcasted_iota(jnp.int32, (rows, width), 1)
    for h in range(heads):
        q_h = q_ref[:, h * width : (h + 1) * width] * jnp.bfloat16(dim**-0.5)
        for m in range(2):
            qs_ref[2 * h + m] = jnp.where((lane >= m * dim) & (lane < (m + 1) * dim), q_h, jnp.bfloat16(0))
    max_ref[...] = jnp.full_like(max_ref, MASKED)
    acc_ref[...] = jnp.zeros_like(acc_ref)

    def visit(block, masked):
        start = pl.multiple_of(block * KEY_BLOCK, KEY_BLOCK)
        key_blk = kv_ref[pl.ds(start, KEY_BLOCK), :width]
        value_blk = kv_ref[pl.ds(start, KEY_BLOCK), width:]
        value_ones = jnp.concatenate([value_blk, jnp.ones_like(value_blk)], axis=1)
        for g in range(2 * heads):
            scores = lax.dot_general(
                qs_ref[g], key_blk, (((1,), (1,)), ((), ())), preferred_element_type=jnp.float32
            )
            if masked:
                key_pos = start + lax.broadcasted_iota(jnp.int32, scores.shape, 1)
                query_pos = first + lax.broadcasted_iota(jnp.int32, scores.shape, 0)
                scores = jnp.where(key_pos <= query_pos, scores, MASKED)
            old_max = max_ref[g]
            new_max = jnp.maximum(old_max, jnp.max(scores, axis=1, keepdims=True))
            shrink = jnp.exp(old_max - new_max)
            weights = jnp.exp(scores - new_max[:, :1]).astype(jnp.bfloat16)
            part = jnp.dot(weights, value_ones, preferred_element_type=jnp.float32)
            acc_ref[g] = acc_ref[g] * jnp.concatenate([shrink, shrink], axis=1) + part
            max_ref[g] = new_max

    full_blocks = first // KEY_BLOCK

    @pl.loop(0, full_blocks)
    def _(block):
        visit(block, False)

    visit(full_blocks, True)
    for h in range(heads):
        one, two = acc_ref[2 * h], acc_ref[2 * h + 1]
        head_out = one[:, :width] / one[:, width:] - lam_ref[h] * (two[:, :width] / two[:, width:])
        mean_sq = jnp.mean(head_out * head_out, axis=1, keepdims=True)
        out_ref[:, h * width : (h + 1) * width] = (
            head_out * lax.rsqrt(mean_sq + EPSILON) * gain_ref[...]
        ).astype(jnp.bfloat16)


def attention(queries, kv, attn_lambda, head_gain, place):
    rows, heads, width = queries.shape
    maps = 2 * heads
    keys = kv.shape[0]
    return pl.pallas_call(
        functools.partial(attention_body, heads=heads, dim=width // 2),
        out_shape=jax.ShapeDtypeStruct((rows, heads * width), jnp.bfloat16),
        in_specs=[
            pl.BlockSpec(memory_space=pltpu.SMEM),
            pl.BlockSpec(memory_space=pltpu.SMEM),
            pl.BlockSpec(memory_space=pltpu.VMEM),
            pl.BlockSpec(memory_space=pltpu.VMEM),
            pl.BlockSpec(memory_space=pltpu.VMEM),
        ],
        out_specs=pl.BlockSpec(memory_space=pltpu.VMEM),
        scratch_shapes=[
            pltpu.VMEM((maps, rows, width), jnp.bfloat16),
            pltpu.VMEM((maps, rows, width), jnp.float32),
            pltpu.VMEM((maps, rows, 2 * width), jnp.float32),
        ],
        cost_estimate=pl.CostEstimate(
            flops=maps * rows * keys * 3 * width * 2,
            bytes_accessed=keys * 2 * width * 2,
            transcendentals=maps * rows * keys,
        ),
        compiler_params=pltpu.CompilerParams(vmem_limit_bytes=32 * 1024 * 1024),
        name="attention",
    )(
        place.reshape(1),
        attn_lambda,
        queries.reshape(rows, heads * width),
        kv,
        head_gain.reshape(1, -1),
    )


def down_body(*refs, hiddens):
    hidden = jnp.concatenate([ref[...] for ref in refs[:hiddens]], axis=1)
    weights = jnp.concatenate([ref[...] for ref in refs[hiddens:-1]], axis=0)
    refs[-1][...] = jnp.dot(hidden, weights, preferred_element_type=jnp.float32).astype(jnp.bfloat16)


def down_product(hidden, weights):
    rows = hidden[0].shape[0]
    width = weights[0].shape[1]
    cols = width // 4
    return pl.pallas_call(
        functools.partial(down_body, hiddens=len(hidden)),
        grid=(width // cols,),
        out_shape=jax.ShapeDtypeStruct((rows, width), jnp.bfloat16),
        in_specs=[pl.BlockSpec(h.shape, lambda n: (0, 0)) for h in hidden]
        + [pl.BlockSpec((w.shape[0], cols), lambda n: (0, n)) for w in weights],
        out_specs=pl.BlockSpec((rows, cols), lambda n: (0, n)),
        cost_estimate=pl.CostEstimate(
            flops=2 * rows * width * sum(w.shape[0] for w in weights),
            bytes_accessed=4 * rows * width,
            transcendentals=0,
        ),
        name="down_product",
    )(*hidden, *weights)


def ring(size, step):
    return [(i, (i + step) % size) for i in range(size)]


def local(
    queries,
    keys,
    values,
    attn_lambda,
    head_gain,
    w_out,
    moe_rows,
    moe_gain,
    routes,
    route_weights,
    w_gate,
    w_up,
    w_down,
):
    tp_count = lax.axis_size("tp")
    tp_id = lax.axis_index("tp")
    experts = lax.axis_size("ep")
    positions, _, _ = queries.shape
    model_width = moe_rows.shape[1]
    dev_rows = moe_rows.shape[0] // tp_count
    top_count = routes.shape[1]
    capacity = max(2, 2 * dev_rows * top_count // experts)
    slots = experts * capacity
    up_ring, down_ring = ring(tp_count, 1), ring(tp_count, -1)

    gate, up = w_gate[0], w_up[0]
    half = w_down.shape[1] // 2
    down = w_down[0]
    downs = [down[:half], down[half:]]

    def send(x, way):
        return lax.ppermute(x, "tp", way)

    gate_a, gate_b = send(gate, up_ring), send(gate, down_ring)
    up_a, up_b = send(up, up_ring), send(up, down_ring)
    gate_c, up_c = send(gate_a, up_ring), send(up_b, down_ring)
    down_parts = []
    for c, x in enumerate(downs):
        near_a, near_b = send(x, up_ring), send(x, down_ring)
        far = send(near_a, up_ring) if c == 0 else send(near_b, down_ring)
        down_parts.append((near_a, near_b, far))

    kv = jnp.concatenate([keys.reshape(positions, -1), values.reshape(positions, -1)], axis=1)
    kv_all = lax.all_gather(kv, "ep", axis=0, tiled=True)

    own_routes = lax.dynamic_slice_in_dim(routes, tp_id * dev_rows, dev_rows, 0)
    own_weights = lax.dynamic_slice_in_dim(route_weights, tp_id * dev_rows, dev_rows, 0)
    rows_f = lax.dynamic_slice_in_dim(moe_rows, tp_id * dev_rows, dev_rows, 0).astype(jnp.float32)
    mean_sq = jnp.mean(rows_f * rows_f, axis=-1, keepdims=True)
    normed = (rows_f * lax.rsqrt(mean_sq + EPSILON) * moe_gain).astype(jnp.bfloat16)
    flat_ids = own_routes.reshape(-1)
    order = lax.iota(jnp.int32, flat_ids.shape[0])
    same = (flat_ids[:, None] == flat_ids[None, :]) & (order[None, :] < order[:, None])
    slot_ids = jnp.sum(same.astype(jnp.int32), axis=1)
    place = (flat_ids * capacity + slot_ids).reshape(dev_rows, top_count)
    slot_range = lax.iota(jnp.int32, slots)
    taken = slot_range[:, None] == place[:, 0][None, :]
    for k in range(1, top_count):
        taken = taken | (slot_range[:, None] == place[:, k][None, :])
    outgoing = jnp.dot(taken.astype(jnp.bfloat16), normed, preferred_element_type=jnp.float32).astype(jnp.bfloat16)
    arrived = lax.all_to_all(
        outgoing.reshape(experts, capacity, model_width), "ep", split_axis=0, concat_axis=0, tiled=True
    ).reshape(slots, model_width)

    def hidden_of(g, u):
        gate_out = jnp.dot(arrived, g, preferred_element_type=jnp.float32)
        up_out = jnp.dot(arrived, u, preferred_element_type=jnp.float32)
        return (jax.nn.silu(gate_out) * up_out).astype(jnp.bfloat16)

    hidden = []
    for g, u in ((gate, up), (gate_a, up_a), (gate_b, up_b), (gate_c, up_c)):
        hidden.append(hidden_of(g, u))

    hit = [(slot_range[None, :] == place[:, k][:, None]).astype(jnp.float32) for k in range(top_count)]
    mix = sum(own_weights[:, k : k + 1] * hit[k] for k in range(top_count))
    mix_hi = mix.astype(jnp.bfloat16)
    mix_lo = (mix - mix_hi.astype(jnp.float32)).astype(jnp.bfloat16)
    near_a, near_b, far = zip(*down_parts)
    out = down_product(hidden, [down, *near_a, *near_b, *far])
    returned = lax.all_to_all(
        out.reshape(experts, capacity, -1), "ep", split_axis=0, concat_axis=0, tiled=True
    ).reshape(slots, -1)
    moe_out = (
        jnp.dot(mix_hi, returned, preferred_element_type=jnp.float32)
        + jnp.dot(mix_lo, returned, preferred_element_type=jnp.float32)
    ).astype(jnp.bfloat16)

    attn_rows = attention(queries, kv_all, attn_lambda, head_gain, lax.axis_index("ep"))
    block = positions // tp_count
    head_width = attn_rows.shape[1]
    mixer_f = jnp.zeros((block, model_width), jnp.float32)
    for step in range(tp_count):
        piece = lax.dynamic_slice_in_dim(attn_rows, (tp_id + step) % tp_count * block, block, 0)
        if step:
            piece = send(piece, ring(tp_count, step))
        w_rows = lax.dynamic_slice_in_dim(w_out, (tp_id - step) % tp_count * head_width, head_width, 0)
        mixer_f = mixer_f + jnp.dot(piece, w_rows, preferred_element_type=jnp.float32)
    mixer_out = mixer_f.astype(jnp.bfloat16)
    return (mixer_out, moe_out)


def solution(mesh):
    return jax.shard_map(
        local,
        mesh=mesh,
        in_specs=(
            P("ep", "tp", None),
            P("ep", "tp", None),
            P("ep", "tp", None),
            P("tp"),
            P(),
            P(),
            P("ep", None),
            P(),
            P("ep", None),
            P("ep", None),
            P("ep", None, "tp"),
            P("ep", None, "tp"),
            P("ep", "tp", None),
        ),
        out_specs=(P(("ep", "tp"), None), P(("ep", "tp"), None)),
        check_vma=False,
    )
```

time: 438 us -> 262 us (0.60)
  the two profiles are of different devices: /device:TPU:2 before, /device:TPU:228 now
where the time goes in v1:
time: 262 us
  waiting for transfers between devices  137 us (52%)
  starting transfers between devices  40.7 us (16%)
  Pallas kernels  38 us (15%)
  matrix products  21.8 us (8%)
  between operations  14.5 us (6%)
  local copies, waits for them, and re-layouts  6.6 us (3%)
  other arithmetic  2.98 us (1%)
    all_to_all x1, waiting for transfers between devices, local(): lax.all_to_all(outgoing.reshape(experts, capacity, model_width), 'ep', sp...  49.9 us
    all_to_all x1, waiting for transfers between devices, local(): lax.all_to_all(out.reshape(experts, capacity, -1), 'ep', split_axis=0, co...  46.7 us
    ppermute x15, waiting for transfers between devices, send(): return lax.ppermute(x, 'tp', way)  40.4 us
    pallas_call x1, Pallas kernels, attention(): pl.pallas_call(functools.partial(attention_body, heads=heads, dim=width /...  31.7 us
    ppermute x15, starting transfers between devices, send(): return lax.ppermute(x, 'tp', way)  21.6 us
    all_to_all x1, starting transfers between devices, local(): lax.all_to_all(out.reshape(experts, capacity, -1), 'ep', split_axis=0, co...  9.91 us
    all_to_all x1, starting transfers between devices, local(): lax.all_to_all(outgoing.reshape(experts, capacity, model_width), 'ep', sp...  9.23 us
    dot_general x4, matrix products, hidden_of(): up_out = jnp.dot(arrived, u, preferred_element_type=jnp.float32)  8.18 us
  transfers between devices with their start and end apart: 18, of which 9 were waited for; matrix products, arithmetic and copies ran while one was open for 9% of the time, Pallas kernels for 2%

profile of v1, /device:TPU:228, one launch (start us, length us, event | category | flops | bytes accessed | tf_op | source)
XLA Modules:
  0.0 261.5 jit_solution(1481981329128296807)
XLA Ops:
  7.2 0.0 copy-start
  7.2 0.0 all-gather.2.cloned.1.call-start
  7.2 1.5 pad_maximum_fusion
  8.8 0.0 all-gather.2.cloned.1.call-update
  8.8 0.1 copy.18
  8.9 0.1 eq.81
  9.1 0.2 convert_reduce_fusion
  9.3 0.1 reduce_sum.21
  9.4 1.2 fusion.29
  10.7 0.2 slice_reduce_fusion.1
  10.9 3.2 %fusion = bf16[64,8,2048]{2,1,0:T(8,128)(2,1)} fusion(f32[2048]{0:T(1024)} %param.20, f32[128]{0:T(128)S(1)} %add_rsqrt_fusion, bf16[512,2048]{1,0:T(8,128)(2,1)} %param.19, s32[]{:T(128)S(6)} %select_n.77, s32[128]{0:T(128)S(1)} %get-tuple-element.3, s32[128]{0:T(128)S(1)} %get-tuple-element.2), kind=kOutput, calls=%fused_computation.1 | convolution fusion | flops 270729216 | bytes 2631172 | tf_op jit(solution)/shard_map/dot_general | solution.py:191
  14.1 9.2 %all-to-all-start = ((bf16[64,8,2048]{2,1,0:T(8,128)(2,1)}), bf16[64,8,2048]{2,1,0:T(8,128)(2,1)S(1)}, u32[]{:S(2)}, u32[]{:S(2)}) async-start(bf16[64,8,2048]{2,1,0:T(8,128)(2,1)} %fusion), calls=%async_computation | async-start | bytes 4194304 | tf_op jit(solution)/shard_map/all_to_all | solution.py:192
  23.3 1.7 collective-permute-start.3
  25.0 1.7 collective-permute-start.5
  26.6 0.4 collective-permute-start.4
  27.0 2.9 %collective-permute-start.6 = (bf16[2048,256]{1,0:T(8,128)(2,1)}, bf16[2048,256]{1,0:T(8,128)(2,1)}, u32[]{:S(2)}, u32[]{:S(2)}) collective-permute-start(bf16[2048,256]{1,0:T(8,128)(2,1)} %bitcast.77), channel_id=1, source_target_pairs={{0,3},{1,0},{2,1},{3,2},{4,7},{5,4},{6,5},{7,6},{8,11},{9,8},{10,9... | collective-permute-start | bytes 3145736 | tf_op jit(solution)/shard_map/ppermute | solution.py:163
  29.9 1.0 slice_bitcast_fusion
  30.9 0.0 collective-permute-start.9
  30.9 49.9 %all-to-all-done = bf16[64,8,2048]{2,1,0:T(8,128)(2,1)S(1)} async-done(((bf16[64,8,2048]{2,1,0:T(8,128)(2,1)}), bf16[64,8,2048]{2,1,0:T(8,128)(2,1)S(1)}, u32[]{:S(2)}, u32[]{:S(2)}) %all-to-all-start) | async-done | bytes 2097184 | tf_op jit(solution)/shard_map/all_to_all | solution.py:192
  80.8 1.9 fusion.21
  82.7 0.0 copy-start.6
  82.8 1.4 fusion.26.refs_0_
  84.2 0.0 collective-permute-done.3
  84.2 2.9 %collective-permute-start.12 = (bf16[128,2048]{1,0:T(8,128)(2,1)S(1)}, bf16[128,2048]{1,0:T(8,128)(2,1)S(1)}, u32[]{:S(2)}, u32[]{:S(2)}) collective-permute-start(bf16[128,2048]{1,0:T(8,128)(2,1)S(1)} %copy-done.6), channel_id=1, source_target_pairs={{0,3},{1,0},{2,1},{3,2},{4,7},{5,4},{6,5},{7,6},{8,11},{9,8},{10,9... | collective-permute-start | bytes 1572872 | tf_op jit(solution)/shard_map/ppermute | solution.py:163
  87.1 0.0 collective-permute-done.5
  87.1 0.0 collective-permute-done.6
  87.1 3.2 %collective-permute-start.8 = (bf16[2048,256]{1,0:T(8,128)(2,1)}, bf16[2048,256]{1,0:T(8,128)(2,1)S(1)}, u32[]{:S(2)}, u32[]{:S(2)}) collective-permute-start(bf16[2048,256]{1,0:T(8,128)(2,1)} %collective-permute-done.6), channel_id=1, source_target_pairs={{0,3},{1,0},{2,1},{3,2},{4,7},{5,4},{6,5},{7,6},{8,11},{9,8},{10,9... | collective-permute-start | bytes 3145736 | tf_op jit(solution)/shard_map/ppermute | solution.py:163
  90.4 2.0 fusion.13
  92.3 2.7 %multiply_convert_fusion.1.refs_2_ = bf16[512,256]{1,0:T(8,128)(2,1)} fusion(f32[512,256]{1,0:T(8,128)S(1)} %fusion.13, bf16[2048,256]{1,0:T(8,128)(2,1)} %collective-permute-done.6, bf16[64,8,2048]{2,1,0:T(8,128)(2,1)S(1)} %all-to-all-done), kind=kOutput, calls=%fused_computation.43 | convolution fusion | flops 537657344 | bytes 3932160 | tf_op jit(solution)/shard_map/dot_general | solution.py:198
  95.0 2.0 fusion.17
  97.0 0.0 collective-permute-done.4
  97.0 0.3 collective-permute-start.10
  97.2 2.7 %multiply_convert_fusion.2.refs_1_ = bf16[512,256]{1,0:T(8,128)(2,1)} fusion(f32[512,256]{1,0:T(8,128)S(1)} %fusion.17, bf16[2048,256]{1,0:T(8,128)(2,1)} %collective-permute-done.4, bf16[64,8,2048]{2,1,0:T(8,128)(2,1)S(1)} %all-to-all-done), kind=kOutput, calls=%fused_computation.44 | convolution fusion | flops 537657344 | bytes 3932160 | tf_op jit(solution)/shard_map/dot_general | solution.py:198
  99.9 3.3 %collective-permute-start.11 = (bf16[128,2048]{1,0:T(8,128)(2,1)}, bf16[128,2048]{1,0:T(8,128)(2,1)S(1)}, u32[]{:S(2)}, u32[]{:S(2)}) collective-permute-start(bf16[128,2048]{1,0:T(8,128)(2,1)} %get-tuple-element.5), channel_id=1, source_target_pairs={{0,3},{1,0},{2,1},{3,2},{4,7},{5,4},{6,5},{7,6},{8,11},{9,8},{10,9... | collective-permute-start | bytes 1572872 | tf_op jit(solution)/shard_map/ppermute | solution.py:163
  103.2 0.0 collective-permute-start.13
  103.2 11.4 %collective-permute-done.7 = bf16[2048,256]{1,0:T(8,128)(2,1)S(1)} collective-permute-done((bf16[2048,256]{1,0:T(8,128)(2,1)}, bf16[2048,256]{1,0:T(8,128)(2,1)S(1)}, u32[]{:S(2)}, u32[]{:S(2)}) %collective-permute-start.7) | collective-permute-done | bytes 1048608 | tf_op jit(solution)/shard_map/ppermute | solution.py:163
  114.6 0.0 collective-permute-start.14
  114.6 0.7 fusion.9
  115.3 6.7 %collective-permute-done.8 = bf16[2048,256]{1,0:T(8,128)(2,1)S(1)} collective-permute-done((bf16[2048,256]{1,0:T(8,128)(2,1)}, bf16[2048,256]{1,0:T(8,128)(2,1)S(1)}, u32[]{:S(2)}, u32[]{:S(2)}) %collective-permute-start.8) | collective-permute-done | bytes 1048608 | tf_op jit(solution)/shard_map/ppermute | solution.py:163
  122.0 1.4 multiply_convert_fusion.refs_3_
  123.4 2.4 collective-permute-done.10.refs_6_
  125.8 7.4 %collective-permute-done.11.refs_7_ = bf16[128,2048]{1,0:T(8,128)(2,1)S(1)} collective-permute-done((bf16[128,2048]{1,0:T(8,128)(2,1)}, bf16[128,2048]{1,0:T(8,128)(2,1)S(1)}, u32[]{:S(2)}, u32[]{:S(2)}) %collective-permute-start.11) | collective-permute-done | bytes 524320 | tf_op jit(solution)/shard_map/ppermute | solution.py:163
  133.2 1.6 collective-permute-done.13.refs_9_
  134.9 7.6 %collective-permute-done.14.refs_10_ = bf16[128,2048]{1,0:T(8,128)(2,1)S(1)} collective-permute-done((bf16[128,2048]{1,0:T(8,128)(2,1)S(1)}, bf16[128,2048]{1,0:T(8,128)(2,1)S(1)}, u32[]{:S(2)}, u32[]{:S(2)}) %collective-permute-start.14) | collective-permute-done | bytes 524320 | tf_op jit(solution)/shard_map/ppermute | solution.py:163
  142.5 0.8 copy-done.13
  143.3 6.3 %down_product.1 = bf16[512,2048]{1,0:T(8,128)(2,1)} custom-call(bf16[512,256]{1,0:T(8,128)(2,1)} %fusion.26.refs_0_, bf16[512,256]{1,0:T(8,128)(2,1)} %multiply_convert_fusion.2.refs_1_, bf16[512,256]{1,0:T(8,128)(2,1)} %multiply_convert_fusion.1.refs_2_, bf16[512,256]{1,0:T(8,128)(2,1)} %multiply_convert_fusion.refs_3_, bf16[256,2048]{1,0:T(8,128)(2,1)} %bitcast.70, ...), custom_call_target="tpu_custom_call" | custom-call | flops 2147483648 | bytes 4194304 | tf_op jit(solution)/shard_map/down_product/pallas_call | solution.py:111
  149.6 9.9 %all-to-all-start.1 = ((bf16[64,8,2048]{2,1,0:T(8,128)(2,1)}), bf16[64,8,2048]{2,1,0:T(8,128)(2,1)S(1)}, u32[]{:S(2)}, u32[]{:S(2)}) async-start(bf16[64,8,2048]{2,1,0:T(8,128)(2,1)} %bitcast.69), calls=%async_computation.1 | async-start | bytes 4194304 | tf_op jit(solution)/shard_map/all_to_all | solution.py:211
  159.7 0.7 constant_dynamic-slice_fusion
  160.4 46.7 %all-to-all-done.1 = bf16[64,8,2048]{2,1,0:T(8,128)(2,1)S(1)} async-done(((bf16[64,8,2048]{2,1,0:T(8,128)(2,1)}), bf16[64,8,2048]{2,1,0:T(8,128)(2,1)S(1)}, u32[]{:S(2)}, u32[]{:S(2)}) %all-to-all-start.1) | async-done | bytes 2097184 | tf_op jit(solution)/shard_map/all_to_all | solution.py:211
  207.1 0.5 fusion.4
  207.6 0.0 copy-start.2
  207.6 0.0 copy-start.3
  207.6 1.3 fusion.1
  209.0 3.4 %copy-done.1 = bf16[16384,256]{1,0:T(8,128)(2,1)S(1)} copy-done((bf16[16384,256]{1,0:T(8,128)(2,1)S(1)}, bf16[16384,256]{1,0:T(8,128)(2,1)}, u32[]{:S(2)}) %copy-start.1) | copy-done | bytes 8388632
  212.3 31.7 %attention.1 = bf16[256,256]{1,0:T(8,128)(2,1)S(1)} custom-call(s32[1]{0:T(128)} %bitcast.place_ref, f32[2]{0:T(128)S(1)} %copy-done.2, bf16[256,256]{1,0:T(8,128)(2,1)S(1)} %bitcast.67, bf16[16384,256]{1,0:T(8,128)(2,1)S(1)} %copy-done.1, f32[1,128]{1,0:T(1,128)S(1)} %bitcast.68), custom_call_target="tpu_custom_call" | custom-call | flops 12884901888 | bytes 8388608 | tf_op jit(solution)/shard_map/attention/pallas_call | solution.py:69
  244.1 3.8 %collective-permute-start.2 = (bf16[64,256]{1,0:T(8,128)(2,1)S(1)}, bf16[64,256]{1,0:T(8,128)(2,1)S(1)}, u32[]{:S(2)}, u32[]{:S(2)}) collective-permute-start(bf16[64,256]{1,0:T(8,128)(2,1)S(1)} %get-tuple-element.7), channel_id=1, source_target_pairs={{0,3},{1,0},{2,1},{3,2},{4,7},{5,4},{6,5},{7,6},{8,11},{9,8},{10,9... | collective-permute-start | bytes 98312 | tf_op jit(solution)/shard_map/ppermute | solution.py:163
  247.9 1.5 collective-permute-start.1
  249.4 0.3 fusion.36
  249.7 3.3 %collective-permute-done = bf16[64,256]{1,0:T(8,128)(2,1)S(1)} collective-permute-done((bf16[64,256]{1,0:T(8,128)(2,1)S(1)}, bf16[64,256]{1,0:T(8,128)(2,1)S(1)}, u32[]{:S(2)}, u32[]{:S(2)}) %collective-permute-start) | collective-permute-done | bytes 32800 | tf_op jit(solution)/shard_map/ppermute | solution.py:163
  253.0 0.3 convolution_add_fusion.2
  253.3 0.0 collective-permute-done.2
  253.3 0.3 fusion.32
  253.6 0.0 collective-permute-done.1
  253.6 1.0 fusion.3
  (33 shorter events, 0.1 us)
Async XLA Ops:
  7.2 1.6 copy-start
  7.2 201.8 %all-gather.2.cloned.1.call-start = ((), (), s32[]{:S(2)}) async-start(), calls=%async_computation.2 | async-start | bytes 8519680 | tf_op jit(solution)/shard_map/all_gather | solution.py:175
  14.1 15.8 %copy-start.5 = (bf16[1,256,2048]{2,1,0:T(8,128)(2,1)S(1)}, bf16[1,256,2048]{2,1,0:T(8,128)(2,1)}, u32[]{:S(2)}) copy-start(bf16[1,256,2048]{2,1,0:T(8,128)(2,1)} %param.25) | copy-start | bytes 3145732
  14.1 66.7 %all-to-all-start = ((bf16[64,8,2048]{2,1,0:T(8,128)(2,1)}), bf16[64,8,2048]{2,1,0:T(8,128)(2,1)S(1)}, u32[]{:S(2)}, u32[]{:S(2)}) async-start(bf16[64,8,2048]{2,1,0:T(8,128)(2,1)} %fusion), calls=%async_computation | async-start | bytes 4194304 | tf_op jit(solution)/shard_map/all_to_all | solution.py:192
  23.3 60.8 %collective-permute-start.3 = (bf16[2048,256]{1,0:T(8,128)(2,1)}, bf16[2048,256]{1,0:T(8,128)(2,1)}, u32[]{:S(2)}, u32[]{:S(2)}) collective-permute-start(bf16[2048,256]{1,0:T(8,128)(2,1)} %bitcast.74), channel_id=1, source_target_pairs={{0,1},{1,2},{2,3},{3,0},{4,5},{5,6},{6,7},{7,4},{8,9},{9,10},{10,1... | collective-permute-start | bytes 3145736 | tf_op jit(solution)/shard_map/ppermute | solution.py:163
  25.0 62.1 %collective-permute-start.5 = (bf16[2048,256]{1,0:T(8,128)(2,1)}, bf16[2048,256]{1,0:T(8,128)(2,1)}, u32[]{:S(2)}, u32[]{:S(2)}) collective-permute-start(bf16[2048,256]{1,0:T(8,128)(2,1)} %bitcast.75), channel_id=1, source_target_pairs={{0,3},{1,0},{2,1},{3,2},{4,7},{5,4},{6,5},{7,6},{8,11},{9,8},{10,9... | collective-permute-start | bytes 3145736 | tf_op jit(solution)/shard_map/ppermute | solution.py:163
  26.6 70.3 %collective-permute-start.4 = (bf16[2048,256]{1,0:T(8,128)(2,1)}, bf16[2048,256]{1,0:T(8,128)(2,1)}, u32[]{:S(2)}, u32[]{:S(2)}) collective-permute-start(bf16[2048,256]{1,0:T(8,128)(2,1)} %bitcast.76), channel_id=1, source_target_pairs={{0,1},{1,2},{2,3},{3,0},{4,5},{5,6},{6,7},{7,4},{8,9},{9,10},{10,1... | collective-permute-start | bytes 3145736 | tf_op jit(solution)/shard_map/ppermute | solution.py:163
  27.0 60.1 %collective-permute-start.6 = (bf16[2048,256]{1,0:T(8,128)(2,1)}, bf16[2048,256]{1,0:T(8,128)(2,1)}, u32[]{:S(2)}, u32[]{:S(2)}) collective-permute-start(bf16[2048,256]{1,0:T(8,128)(2,1)} %bitcast.77), channel_id=1, source_target_pairs={{0,3},{1,0},{2,1},{3,2},{4,7},{5,4},{6,5},{7,6},{8,11},{9,8},{10,9... | collective-permute-start | bytes 3145736 | tf_op jit(solution)/shard_map/ppermute | solution.py:163
  30.9 51.8 %copy-start.8 = (bf16[1,2048,256]{2,1,0:T(8,128)(2,1)S(1)}, bf16[1,2048,256]{2,1,0:T(8,128)(2,1)}, u32[]{:S(2)}) copy-start(bf16[1,2048,256]{2,1,0:T(8,128)(2,1)} %param.24) | copy-start | bytes 3145732
  30.9 69.0 %collective-permute-start.9 = (bf16[128,2048]{1,0:T(8,128)(2,1)}, bf16[128,2048]{1,0:T(8,128)(2,1)}, u32[]{:S(2)}, u32[]{:S(2)}) collective-permute-start(bf16[128,2048]{1,0:T(8,128)(2,1)} %get-tuple-element.5), channel_id=1, source_target_pairs={{0,1},{1,2},{2,3},{3,0},{4,5},{5,6},{6,7},{7,4},{8,9},{9,10},{10,1... | collective-permute-start | bytes 1572872 | tf_op jit(solution)/shard_map/ppermute | solution.py:163
  82.7 1.4 copy-start.6
  84.2 19.0 %collective-permute-start.12 = (bf16[128,2048]{1,0:T(8,128)(2,1)S(1)}, bf16[128,2048]{1,0:T(8,128)(2,1)S(1)}, u32[]{:S(2)}, u32[]{:S(2)}) collective-permute-start(bf16[128,2048]{1,0:T(8,128)(2,1)S(1)} %copy-done.6), channel_id=1, source_target_pairs={{0,3},{1,0},{2,1},{3,2},{4,7},{5,4},{6,5},{7,6},{8,11},{9,8},{10,9... | collective-permute-start | bytes 1572872 | tf_op jit(solution)/shard_map/ppermute | solution.py:163
  87.1 27.5 %collective-permute-start.7 = (bf16[2048,256]{1,0:T(8,128)(2,1)}, bf16[2048,256]{1,0:T(8,128)(2,1)S(1)}, u32[]{:S(2)}, u32[]{:S(2)}) collective-permute-start(bf16[2048,256]{1,0:T(8,128)(2,1)} %collective-permute-done.3), channel_id=1, source_target_pairs={{0,1},{1,2},{2,3},{3,0},{4,5},{5,6},{6,7},{7,4},{8,9},{9,10},{10,1... | collective-permute-start | bytes 3145736 | tf_op jit(solution)/shard_map/ppermute | solution.py:163
  87.1 34.9 %collective-permute-start.8 = (bf16[2048,256]{1,0:T(8,128)(2,1)}, bf16[2048,256]{1,0:T(8,128)(2,1)S(1)}, u32[]{:S(2)}, u32[]{:S(2)}) collective-permute-start(bf16[2048,256]{1,0:T(8,128)(2,1)} %collective-permute-done.6), channel_id=1, source_target_pairs={{0,3},{1,0},{2,1},{3,2},{4,7},{5,4},{6,5},{7,6},{8,11},{9,8},{10,9... | collective-permute-start | bytes 3145736 | tf_op jit(solution)/shard_map/ppermute | solution.py:163
  97.0 28.8 %collective-permute-start.10 = (bf16[128,2048]{1,0:T(8,128)(2,1)S(1)}, bf16[128,2048]{1,0:T(8,128)(2,1)S(1)}, u32[]{:S(2)}, u32[]{:S(2)}) collective-permute-start(bf16[128,2048]{1,0:T(8,128)(2,1)S(1)} %copy-done.6), channel_id=1, source_target_pairs={{0,1},{1,2},{2,3},{3,0},{4,5},{5,6},{6,7},{7,4},{8,9},{9,10},{10,1... | collective-permute-start | bytes 1572872 | tf_op jit(solution)/shard_map/ppermute | solution.py:163
  99.9 33.3 %collective-permute-start.11 = (bf16[128,2048]{1,0:T(8,128)(2,1)}, bf16[128,2048]{1,0:T(8,128)(2,1)S(1)}, u32[]{:S(2)}, u32[]{:S(2)}) collective-permute-start(bf16[128,2048]{1,0:T(8,128)(2,1)} %get-tuple-element.5), channel_id=1, source_target_pairs={{0,3},{1,0},{2,1},{3,2},{4,7},{5,4},{6,5},{7,6},{8,11},{9,8},{10,9... | collective-permute-start | bytes 1572872 | tf_op jit(solution)/shard_map/ppermute | solution.py:163
  103.2 20.2 %copy-start.9 = (bf16[128,2048]{1,0:T(8,128)(2,1)}, bf16[128,2048]{1,0:T(8,128)(2,1)S(1)}, u32[]{:S(2)}) copy-start(bf16[128,2048]{1,0:T(8,128)(2,1)S(1)} %collective-permute-done.12.refs_8_) | copy-start | bytes 1572868
  103.2 31.7 %collective-permute-start.13 = (bf16[128,2048]{1,0:T(8,128)(2,1)}, bf16[128,2048]{1,0:T(8,128)(2,1)S(1)}, u32[]{:S(2)}, u32[]{:S(2)}) collective-permute-start(bf16[128,2048]{1,0:T(8,128)(2,1)} %collective-permute-done.9.refs_5_), channel_id=1, source_target_pairs={{0,1},{1,2},{2,3},{3,0},{4,5},{5,6},{6,7},{7,4},{8,9},{9,10},{10,1... | collective-permute-start | bytes 1572872 | tf_op jit(solution)/shard_map/ppermute | solution.py:163
  114.6 27.9 %collective-permute-start.14 = (bf16[128,2048]{1,0:T(8,128)(2,1)S(1)}, bf16[128,2048]{1,0:T(8,128)(2,1)S(1)}, u32[]{:S(2)}, u32[]{:S(2)}) collective-permute-start(bf16[128,2048]{1,0:T(8,128)(2,1)S(1)} %collective-permute-done.12.refs_8_), channel_id=1, source_target_pairs={{0,3},{1,0},{2,1},{3,2},{4,7},{5,4},{6,5},{7,6},{8,11},{9,8},{10,9... | collective-permute-start | bytes 1572872 | tf_op jit(solution)/shard_map/ppermute | solution.py:163
  125.8 17.5 %copy-start.10 = (bf16[128,2048]{1,0:T(8,128)(2,1)}, bf16[128,2048]{1,0:T(8,128)(2,1)S(1)}, u32[]{:S(2)}) copy-start(bf16[128,2048]{1,0:T(8,128)(2,1)S(1)} %collective-permute-done.10.refs_6_) | copy-start | bytes 1572868
  133.2 9.2 %copy-start.11 = (bf16[128,2048]{1,0:T(8,128)(2,1)}, bf16[128,2048]{1,0:T(8,128)(2,1)S(1)}, u32[]{:S(2)}) copy-start(bf16[128,2048]{1,0:T(8,128)(2,1)S(1)} %collective-permute-done.11.refs_7_) | copy-start | bytes 1572868
  134.9 7.6 %copy-start.12 = (bf16[128,2048]{1,0:T(8,128)(2,1)}, bf16[128,2048]{1,0:T(8,128)(2,1)S(1)}, u32[]{:S(2)}) copy-start(bf16[128,2048]{1,0:T(8,128)(2,1)S(1)} %collective-permute-done.13.refs_9_) | copy-start | bytes 1572868
  142.5 0.8 copy-start.13
  149.6 10.0 %copy-start.7 = (bf16[256,2,128]{2,1,0:T(2,128)(2,1)S(1)}, bf16[256,2,128]{2,1,0:T(2,128)(2,1)}, u32[]{:S(2)}) copy-start(bf16[256,2,128]{2,1,0:T(2,128)(2,1)} %param.13) | copy-start | bytes 393220
  149.6 57.5 %all-to-all-start.1 = ((bf16[64,8,2048]{2,1,0:T(8,128)(2,1)}), bf16[64,8,2048]{2,1,0:T(8,128)(2,1)S(1)}, u32[]{:S(2)}, u32[]{:S(2)}) async-start(bf16[64,8,2048]{2,1,0:T(8,128)(2,1)} %bitcast.69), calls=%async_computation.1 | async-start | bytes 4194304 | tf_op jit(solution)/shard_map/all_to_all | solution.py:211
  207.6 1.4 copy-start.2
  207.6 1.3 copy-start.3
  209.0 3.4 %copy-start.1 = (bf16[16384,256]{1,0:T(8,128)(2,1)S(1)}, bf16[16384,256]{1,0:T(8,128)(2,1)}, u32[]{:S(2)}) copy-start(bf16[16384,256]{1,0:T(8,128)(2,1)} %all-gather.2.cloned.1.call-done.kv_ref) | copy-start | bytes 25165828
  212.3 37.1 %copy-start.4 = (bf16[1024,2048]{1,0:T(8,128)(2,1)S(1)}, bf16[1024,2048]{1,0:T(8,128)(2,1)}, u32[]{:S(2)}) copy-start(bf16[1024,2048]{1,0:T(8,128)(2,1)} %param.18) | copy-start | bytes 12582916
  244.1 9.2 %collective-permute-start.2 = (bf16[64,256]{1,0:T(8,128)(2,1)S(1)}, bf16[64,256]{1,0:T(8,128)(2,1)S(1)}, u32[]{:S(2)}, u32[]{:S(2)}) collective-permute-start(bf16[64,256]{1,0:T(8,128)(2,1)S(1)} %get-tuple-element.7), channel_id=1, source_target_pairs={{0,3},{1,0},{2,1},{3,2},{4,7},{5,4},{6,5},{7,6},{8,11},{9,8},{10,9... | collective-permute-start | bytes 98312 | tf_op jit(solution)/shard_map/ppermute | solution.py:163
  247.9 5.1 %collective-permute-start = (bf16[64,256]{1,0:T(8,128)(2,1)S(1)}, bf16[64,256]{1,0:T(8,128)(2,1)S(1)}, u32[]{:S(2)}, u32[]{:S(2)}) collective-permute-start(bf16[64,256]{1,0:T(8,128)(2,1)S(1)} %get-tuple-element.8), channel_id=1, source_target_pairs={{0,1},{1,2},{2,3},{3,0},{4,5},{5,6},{6,7},{7,4},{8,9},{9,10},{10,1... | collective-permute-start | bytes 98312 | tf_op jit(solution)/shard_map/ppermute | solution.py:163
  247.9 5.8 %collective-permute-start.1 = (bf16[64,256]{1,0:T(8,128)(2,1)S(1)}, bf16[64,256]{1,0:T(8,128)(2,1)S(1)}, u32[]{:S(2)}, u32[]{:S(2)}) collective-permute-start(bf16[64,256]{1,0:T(8,128)(2,1)S(1)} %get-tuple-element.6), channel_id=1, source_target_pairs={{0,2},{1,3},{2,0},{3,1},{4,6},{5,7},{6,4},{7,5},{8,10},{9,11},{10,... | collective-permute-start | bytes 98312 | tf_op jit(solution)/shard_map/ppermute | solution.py:163
Sparse Core Ops, SparseCore 0:
  10.8 90.6 all-gather.1

commit v2 on v1

--- a/solution.py
+++ b/solution.py
@@ -10,13 +10,23 @@
 
 EPSILON = 1e-06
 MASKED = -1e30
-KEY_BLOCK = 1024
-
-
-def attention_body(place_ref, lam_ref, q_ref, kv_ref, gain_ref, out_ref, qs_ref, max_ref, acc_ref, *, heads, dim):
+EP_SIZES = (8, 4, 2)
+
+
+def attention_body(place_ref, lam_ref, q_ref, gain_ref, *refs, heads, dim):
+    _, x_size, cores = EP_SIZES
+    count = x_size * cores
+    piece_refs = refs[:count]
+    out_ref, kv_ref, sems, qs_ref, max_ref, acc_ref = refs[count:]
+    copies = [pltpu.make_async_copy(piece_refs[i], kv_ref.at[i], sems.at[i]) for i in range(count)]
+    for copy in copies:
+        copy.start()
     rows = q_ref.shape[0]
     width = 2 * dim
-    first = place_ref[0] * rows
+    me = place_ref[0]
+    core = me % cores
+    x = (me // cores) % x_size
+    z = me // (cores * x_size)
     lane = lax.broadcasted_iota(jnp.int32, (rows, width), 1)
     for h in range(heads):
         q_h = q_ref[:, h * width : (h + 1) * width] * jnp.bfloat16(dim**-0.5)
@@ -24,35 +34,44 @@
             qs_ref[2 * h + m] = jnp.where((lane >= m * dim) & (lane < (m + 1) * dim), q_h, jnp.bfloat16(0))
     max_ref[...] = jnp.full_like(max_ref, MASKED)
     acc_ref[...] = jnp.zeros_like(acc_ref)
-
-    def visit(block, masked):
-        start = pl.multiple_of(block * KEY_BLOCK, KEY_BLOCK)
-        key_blk = kv_ref[pl.ds(start, KEY_BLOCK), :width]
-        value_blk = kv_ref[pl.ds(start, KEY_BLOCK), width:]
+    for copy in copies:
+        copy.wait()
+
+    def visit(pieces, offset, places):
+        key_blk = jnp.concatenate([kv_ref[p, pl.ds(offset, rows), :width] for p in pieces], axis=0)
+        value_blk = jnp.concatenate([kv_ref[p, pl.ds(offset, rows), width:] for p in pieces], axis=0)
         value_ones = jnp.concatenate([value_blk, jnp.ones_like(value_blk)], axis=1)
         for g in range(2 * heads):
             scores = lax.dot_general(
                 qs_ref[g], key_blk, (((1,), (1,)), ((), ())), preferred_element_type=jnp.float32
             )
-            if masked:
-                key_pos = start + lax.broadcasted_iota(jnp.int32, scores.shape, 1)
-                query_pos = first + lax.broadcasted_iota(jnp.int32, scores.shape, 0)
-                scores = jnp.where(key_pos <= query_pos, scores, MASKED)
+            if places is not None:
+                shape = (rows, rows)
+                query_pos = me * rows + lax.broadcasted_iota(jnp.int32, shape, 0)
+                key_pos = lax.broadcasted_iota(jnp.int32, shape, 1)
+                first_key = jnp.concatenate([place * rows + key_pos for place in places], axis=1)
+                allowed = first_key <= jnp.concatenate([query_pos] * len(places), axis=1)
+                scores = jnp.where(allowed, scores, MASKED)
             old_max = max_ref[g]
             new_max = jnp.maximum(old_max, jnp.max(scores, axis=1, keepdims=True))
             shrink = jnp.exp(old_max - new_max)
-            weights = jnp.exp(scores - new_max[:, :1]).astype(jnp.bfloat16)
+            spread_max = jnp.concatenate([new_max] * (scores.shape[1] // width), axis=1)
+            weights = jnp.exp(scores - spread_max).astype(jnp.bfloat16)
             part = jnp.dot(weights, value_ones, preferred_element_type=jnp.float32)
             acc_ref[g] = acc_ref[g] * jnp.concatenate([shrink, shrink], axis=1) + part
             max_ref[g] = new_max
 
-    full_blocks = first // KEY_BLOCK
-
-    @pl.loop(0, full_blocks)
-    def _(block):
-        visit(block, False)
-
-    visit(full_blocks, True)
+    @pl.loop(0, x + 1)
+    def _(dx):
+        first = (z * x_size + x - dx) * cores
+        visit((dx, x_size + dx), 0, (first + core, first + 1 - core))
+
+    @pl.loop(0, z * cores)
+    def _(step):
+        offset = pl.multiple_of((step // cores + 1) * rows, rows)
+        first = step % cores * x_size
+        visit([first + dx for dx in range(x_size)], offset, None)
+
     for h in range(heads):
         one, two = acc_ref[2 * h], acc_ref[2 * h + 1]
         head_out = one[:, :width] / one[:, width:] - lam_ref[h] * (two[:, :width] / two[:, width:])
@@ -62,22 +81,21 @@
         ).astype(jnp.bfloat16)
 
 
-def attention(queries, kv, attn_lambda, head_gain, place):
+def attention(queries, pieces, attn_lambda, head_gain, place):
     rows, heads, width = queries.shape
     maps = 2 * heads
-    keys = kv.shape[0]
+    count = len(pieces)
+    keys = count * pieces[0].shape[0]
     return pl.pallas_call(
         functools.partial(attention_body, heads=heads, dim=width // 2),
         out_shape=jax.ShapeDtypeStruct((rows, heads * width), jnp.bfloat16),
-        in_specs=[
-            pl.BlockSpec(memory_space=pltpu.SMEM),
-            pl.BlockSpec(memory_space=pltpu.SMEM),
-            pl.BlockSpec(memory_space=pltpu.VMEM),
-            pl.BlockSpec(memory_space=pltpu.VMEM),
-            pl.BlockSpec(memory_space=pltpu.VMEM),
-        ],
+        in_specs=[pl.BlockSpec(memory_space=pltpu.SMEM)] * 2
+        + [pl.BlockSpec(memory_space=pltpu.VMEM)] * 2
+        + [pl.BlockSpec(memory_space=pltpu.HBM)] * count,
         out_specs=pl.BlockSpec(memory_space=pltpu.VMEM),
         scratch_shapes=[
+            pltpu.VMEM((count, *pieces[0].shape), jnp.bfloat16),
+            pltpu.SemaphoreType.DMA((count,)),
             pltpu.VMEM((maps, rows, width), jnp.bfloat16),
             pltpu.VMEM((maps, rows, width), jnp.float32),
             pltpu.VMEM((maps, rows, 2 * width), jnp.float32),
@@ -87,41 +105,89 @@
             bytes_accessed=keys * 2 * width * 2,
             transcendentals=maps * rows * keys,
         ),
+        compiler_params=pltpu.CompilerParams(vmem_limit_bytes=40 * 1024 * 1024),
+        name="attention",
+    )(place.reshape(1), attn_lambda, queries.reshape(rows, heads * width), head_gain.reshape(1, -1), *pieces)
+
+
+def hidden_body(rows_hbm, *refs, shards):
+    weight_refs = refs[: 2 * shards]
+    out_ref, rows_ref, weights_ref, rows_sem, sems = refs[2 * shards :]
+    rows_copy = pltpu.make_async_copy(rows_hbm, rows_ref, rows_sem)
+    rows_copy.start()
+    copies = [pltpu.make_async_copy(weight_refs[i], weights_ref.at[i], sems.at[i]) for i in range(2 * shards)]
+    for copy in copies:
+        copy.start()
+    count = rows_ref.shape[0]
+    block = count // 2
+    rows_copy.wait()
+    for shard in range(shards):
+        copies[2 * shard].wait()
+        copies[2 * shard + 1].wait()
+
+        @pl.loop(0, count // block)
+        def _(step):
+            start = pl.multiple_of(step * block, block)
+            rows = rows_ref[pl.ds(start, block), :]
+            gate_out = jnp.dot(rows, weights_ref[2 * shard], preferred_element_type=jnp.float32)
+            up_out = jnp.dot(rows, weights_ref[2 * shard + 1], preferred_element_type=jnp.float32)
+            out_ref[shard, pl.ds(start, block), :] = (jax.nn.silu(gate_out) * up_out).astype(jnp.bfloat16)
+
+
+def hidden_units(rows, weights):
+    count, depth = rows.shape
+    units = weights[0][0].shape[1]
+    shards = len(weights)
+    flat = [w for pair in weights for w in pair]
+    return pl.pallas_call(
+        functools.partial(hidden_body, shards=shards),
+        out_shape=jax.ShapeDtypeStruct((shards, count, units), jnp.bfloat16),
+        in_specs=[pl.BlockSpec(memory_space=pltpu.HBM)] * (1 + len(flat)),
+        out_specs=pl.BlockSpec(memory_space=pltpu.VMEM),
+        scratch_shapes=[
+            pltpu.VMEM((count, depth), jnp.bfloat16),
+            pltpu.VMEM((len(flat), depth, units), jnp.bfloat16),
+            pltpu.SemaphoreType.DMA,
+            pltpu.SemaphoreType.DMA((len(flat),)),
+        ],
+        cost_estimate=pl.CostEstimate(
+            flops=4 * count * depth * units * shards,
+            bytes_accessed=2 * depth * (count + 2 * units * shards),
+            transcendentals=count * units * shards,
+        ),
         compiler_params=pltpu.CompilerParams(vmem_limit_bytes=32 * 1024 * 1024),
-        name="attention",
-    )(
-        place.reshape(1),
-        attn_lambda,
-        queries.reshape(rows, heads * width),
-        kv,
-        head_gain.reshape(1, -1),
-    )
-
-
-def down_body(*refs, hiddens):
-    hidden = jnp.concatenate([ref[...] for ref in refs[:hiddens]], axis=1)
-    weights = jnp.concatenate([ref[...] for ref in refs[hiddens:-1]], axis=0)
-    refs[-1][...] = jnp.dot(hidden, weights, preferred_element_type=jnp.float32).astype(jnp.bfloat16)
-
-
-def down_product(hidden, weights):
-    rows = hidden[0].shape[0]
+        name="hidden_units",
+    )(rows, *flat)
+
+
+def down_body(hidden_ref, *refs, parts, begun):
+    hidden = jnp.concatenate([hidden_ref[k] for k in range(hidden_ref.shape[0])], axis=1)
+    weights = jnp.concatenate([ref[...] for ref in refs[:parts]], axis=0)
+    total = jnp.dot(hidden, weights, preferred_element_type=jnp.float32)
+    if begun:
+        total = total + refs[parts][...]
+    refs[-1][...] = total.astype(refs[-1].dtype)
+
+
+def down_product(hidden, shards, weights, begun, kind):
+    _, rows, units = hidden.shape
     width = weights[0].shape[1]
     cols = width // 4
+    depth = sum(w.shape[0] for w in weights)
+    first = shards[0] // len(shards)
     return pl.pallas_call(
-        functools.partial(down_body, hiddens=len(hidden)),
+        functools.partial(down_body, parts=len(weights), begun=len(begun)),
         grid=(width // cols,),
-        out_shape=jax.ShapeDtypeStruct((rows, width), jnp.bfloat16),
-        in_specs=[pl.BlockSpec(h.shape, lambda n: (0, 0)) for h in hidden]
-        + [pl.BlockSpec((w.shape[0], cols), lambda n: (0, n)) for w in weights],
+        out_shape=jax.ShapeDtypeStruct((rows, width), kind),
+        in_specs=[pl.BlockSpec((len(shards), rows, units), lambda n: (first, 0, 0))]
+        + [pl.BlockSpec((w.shape[0], cols), lambda n: (0, n)) for w in weights]
+        + [pl.BlockSpec((rows, cols), lambda n: (0, n)) for _ in begun],
         out_specs=pl.BlockSpec((rows, cols), lambda n: (0, n)),
         cost_estimate=pl.CostEstimate(
-            flops=2 * rows * width * sum(w.shape[0] for w in weights),
-            bytes_accessed=4 * rows * width,
-            transcendentals=0,
+            flops=2 * rows * width * depth, bytes_accessed=4 * rows * width, transcendentals=0
         ),
         name="down_product",
-    )(*hidden, *weights)
+    )(hidden, *weights, *begun)
 
 
 def ring(size, step):
@@ -171,8 +237,23 @@
         far = send(near_a, up_ring) if c == 0 else send(near_b, down_ring)
         down_parts.append((near_a, near_b, far))
 
+    z_size, x_size, cores = EP_SIZES
+
+    def ep_shift(dz, dx, dc):
+        pairs = []
+        for i in range(experts):
+            z, x, c = i // (x_size * cores), i // cores % x_size, i % cores
+            to = ((z + dz) % z_size * x_size + (x + dx) % x_size) * cores + (c + dc) % cores
+            pairs.append((i, to))
+        return pairs
+
+    def spread(x, shift):
+        return lax.ppermute(x, "ep", ep_shift(*shift))
+
     kv = jnp.concatenate([keys.reshape(positions, -1), values.reshape(positions, -1)], axis=1)
-    kv_all = lax.all_gather(kv, "ep", axis=0, tiled=True)
+    column = jnp.concatenate([kv] + [spread(kv, (d, 0, 0)) for d in range(1, z_size)], axis=0)
+    own_pieces = [column] + [spread(column, (0, d, 0)) for d in range(1, x_size)]
+    other_pieces = [spread(piece, (0, 0, 1)) for piece in own_pieces]
 
     own_routes = lax.dynamic_slice_in_dim(routes, tp_id * dev_rows, dev_rows, 0)
     own_weights = lax.dynamic_slice_in_dim(route_weights, tp_id * dev_rows, dev_rows, 0)
@@ -193,30 +274,19 @@
         outgoing.reshape(experts, capacity, model_width), "ep", split_axis=0, concat_axis=0, tiled=True
     ).reshape(slots, model_width)
 
-    def hidden_of(g, u):
-        gate_out = jnp.dot(arrived, g, preferred_element_type=jnp.float32)
-        up_out = jnp.dot(arrived, u, preferred_element_type=jnp.float32)
-        return (jax.nn.silu(gate_out) * up_out).astype(jnp.bfloat16)
-
-    hidden = []
-    for g, u in ((gate, up), (gate_a, up_a), (gate_b, up_b), (gate_c, up_c)):
-        hidden.append(hidden_of(g, u))
+    hidden = hidden_units(arrived, [(gate, up), (gate_a, up_a), (gate_b, up_b), (gate_c, up_c)])
 
     hit = [(slot_range[None, :] == place[:, k][:, None]).astype(jnp.float32) for k in range(top_count)]
     mix = sum(own_weights[:, k : k + 1] * hit[k] for k in range(top_count))
-    mix_hi = mix.astype(jnp.bfloat16)
-    mix_lo = (mix - mix_hi.astype(jnp.float32)).astype(jnp.bfloat16)
     near_a, near_b, far = zip(*down_parts)
-    out = down_product(hidden, [down, *near_a, *near_b, *far])
+    begun = down_product(hidden, (0, 1, 2), [down, *near_a, *near_b], [], jnp.float32)
+    out = down_product(hidden, (3,), far, [begun], jnp.bfloat16)
     returned = lax.all_to_all(
         out.reshape(experts, capacity, -1), "ep", split_axis=0, concat_axis=0, tiled=True
     ).reshape(slots, -1)
-    moe_out = (
-        jnp.dot(mix_hi, returned, preferred_element_type=jnp.float32)
-        + jnp.dot(mix_lo, returned, preferred_element_type=jnp.float32)
-    ).astype(jnp.bfloat16)
-
-    attn_rows = attention(queries, kv_all, attn_lambda, head_gain, lax.axis_index("ep"))
+    moe_out = jnp.dot(mix.astype(jnp.bfloat16), returned, preferred_element_type=jnp.float32).astype(jnp.bfloat16)
+
+    attn_rows = attention(queries, own_pieces + other_pieces, attn_lambda, head_gain, lax.axis_index("ep"))
     block = positions // tp_count
     head_width = attn_rows.shape[1]
     mixer_f = jnp.zeros((block, model_width), jnp.float32)

time: 262 us -> 280 us (1.069)
  the two profiles are of different devices: /device:TPU:228 before, /device:TPU:2 now
where the time goes in v2:
time: 280 us; the launch traced here: 279 us
  waiting for transfers between devices  145 us (52%)
  starting transfers between devices  76.2 us (27%)
  Pallas kernels  23.3 us (8%)
  local copies, waits for them, and re-layouts  19 us (7%)
  matrix products  12.9 us (5%)
    ppermute x14, waiting for transfers between devices, spread(): return lax.ppermute(x, 'ep', ep_shift(*shift))  70.4 us
    ppermute x15, waiting for transfers between devices, send(): return lax.ppermute(x, 'tp', way)  48.7 us
    ppermute x14, starting transfers between devices, spread(): return lax.ppermute(x, 'ep', ep_shift(*shift))  28.5 us
    ppermute x15, starting transfers between devices, send(): return lax.ppermute(x, 'tp', way)  26.1 us
    all_to_all x1, waiting for transfers between devices, local(): lax.all_to_all(out.reshape(experts, capacity, -1), 'ep', split_axis=0, co...  25.8 us
    unnamed x58, local copies, waits for them, and re-layouts  16.5 us
    all_to_all x1, starting transfers between devices, local(): lax.all_to_all(outgoing.reshape(experts, capacity, model_width), 'ep', sp...  12.1 us
    pallas_call x2, Pallas kernels, down_product(): pl.pallas_call(functools.partial(down_body, parts=len(weights), begun=len...  11.1 us
  transfers between devices with their start and end apart: 31, of which 15 were waited for; matrix products, arithmetic and copies ran while one was open for 3% of the time, Pallas kernels for 8%

profile of v2, /device:TPU:2, one launch (start us, length us, event | category | flops | bytes accessed | tf_op | source)
XLA Modules:
  0.0 278.7 jit_solution(11310678673950888300)
XLA Ops:
  2.1 1.2 fusion.5
  3.4 3.2 %fusion = bf16[64,8,2048]{2,1,0:T(8,128)(2,1)} fusion(f32[2048]{0:T(1024)} %param.20, f32[128]{0:T(128)S(1)} %add_rsqrt_fusion, bf16[512,2048]{1,0:T(8,128)(2,1)} %param.19, s32[]{:T(128)S(6)} %select_n.77, s32[128]{0:T(128)S(1)} %get-tuple-element.3, s32[128]{0:T(128)S(1)} %get-tuple-element.2), kind=kOutput, calls=%fused_computation.1 | convolution fusion | flops 270729216 | bytes 2631172 | tf_op jit(solution)/shard_map/dot_general | solution.py:272
  6.6 12.1 %all-to-all-start = ((bf16[64,8,2048]{2,1,0:T(8,128)(2,1)}), bf16[64,8,2048]{2,1,0:T(8,128)(2,1)S(1)}, u32[]{:S(2)}, u32[]{:S(2)}) async-start(bf16[64,8,2048]{2,1,0:T(8,128)(2,1)} %fusion), calls=%async_computation | async-start | bytes 4194304 | tf_op jit(solution)/shard_map/all_to_all | solution.py:273
  18.8 1.5 collective-permute-start
  20.3 1.6 collective-permute-start.17
  21.9 1.7 collective-permute-start.20
  23.6 2.4 collective-permute-start.1
  26.0 2.8 %collective-permute-start.2 = (bf16[256,256]{1,0:T(8,128)(2,1)S(1)}, bf16[256,256]{1,0:T(8,128)(2,1)S(1)}, u32[]{:S(2)}, u32[]{:S(2)}) collective-permute-start(bf16[256,256]{1,0:T(8,128)(2,1)S(1)} %get-tuple-element.9), channel_id=1, source_target_pairs={{0,96},{4,100},{8,104},{12,108},{16,112},{20,116},{24,120},{28,124... | collective-permute-start | bytes 393224 | tf_op jit(solution)/shard_map/ppermute | solution.py:251
  28.8 42.3 %collective-permute-done = bf16[256,256]{1,0:T(8,128)(2,1)S(1)} collective-permute-done((bf16[256,256]{1,0:T(8,128)(2,1)S(1)}, bf16[256,256]{1,0:T(8,128)(2,1)S(1)}, u32[]{:S(2)}, u32[]{:S(2)}) %collective-permute-start) | collective-permute-done | bytes 131104 | tf_op jit(solution)/shard_map/ppermute | solution.py:251
  71.1 4.8 %collective-permute-start.3 = (bf16[256,256]{1,0:T(8,128)(2,1)S(1)}, bf16[256,256]{1,0:T(8,128)(2,1)S(1)}, u32[]{:S(2)}, u32[]{:S(2)}) collective-permute-start(bf16[256,256]{1,0:T(8,128)(2,1)S(1)} %get-tuple-element.9), channel_id=1, source_target_pairs={{0,128},{4,132},{8,136},{12,140},{16,144},{20,148},{24,152},{28,15... | collective-permute-start | bytes 393224 | tf_op jit(solution)/shard_map/ppermute | solution.py:251
  75.9 1.3 slice_bitcast_fusion
  77.1 1.0 collective-permute-done.1
  78.1 1.6 collective-permute-start.23
  79.7 7.2 %collective-permute-done.2 = bf16[256,256]{1,0:T(8,128)(2,1)S(1)} collective-permute-done((bf16[256,256]{1,0:T(8,128)(2,1)S(1)}, bf16[256,256]{1,0:T(8,128)(2,1)S(1)}, u32[]{:S(2)}, u32[]{:S(2)}) %collective-permute-start.2) | collective-permute-done | bytes 131104 | tf_op jit(solution)/shard_map/ppermute | solution.py:251
  86.9 3.0 %collective-permute-start.25 = (bf16[128,2048]{1,0:T(8,128)(2,1)S(1)}, bf16[128,2048]{1,0:T(8,128)(2,1)}, u32[]{:S(2)}, u32[]{:S(2)}) collective-permute-start(bf16[128,2048]{1,0:T(8,128)(2,1)S(1)} %get-tuple-element.4), channel_id=1, source_target_pairs={{0,3},{1,0},{2,1},{3,2},{4,7},{5,4},{6,5},{7,6},{8,11},{9,8},{10,9... | collective-permute-start | bytes 1572872 | tf_op jit(solution)/shard_map/ppermute | solution.py:229
  90.5 1.6 collective-permute-start.4
  92.1 6.8 %collective-permute-done.4 = bf16[256,256]{1,0:T(8,128)(2,1)S(1)} collective-permute-done((bf16[256,256]{1,0:T(8,128)(2,1)S(1)}, bf16[256,256]{1,0:T(8,128)(2,1)S(1)}, u32[]{:S(2)}, u32[]{:S(2)}) %collective-permute-start.4) | collective-permute-done | bytes 131104 | tf_op jit(solution)/shard_map/ppermute | solution.py:251
  98.9 8.7 %collective-permute-start.5 = (bf16[256,256]{1,0:T(8,128)(2,1)S(1)}, bf16[256,256]{1,0:T(8,128)(2,1)S(1)}, u32[]{:S(2)}, u32[]{:S(2)}) collective-permute-start(bf16[256,256]{1,0:T(8,128)(2,1)S(1)} %get-tuple-element.9), channel_id=1, source_target_pairs={{0,192},{4,196},{8,200},{12,204},{16,208},{20,212},{24,216},{28,22... | collective-permute-start | bytes 393224 | tf_op jit(solution)/shard_map/ppermute | solution.py:251
  107.6 2.8 %collective-permute-done.5 = bf16[256,256]{1,0:T(8,128)(2,1)S(1)} collective-permute-done((bf16[256,256]{1,0:T(8,128)(2,1)S(1)}, bf16[256,256]{1,0:T(8,128)(2,1)S(1)}, u32[]{:S(2)}, u32[]{:S(2)}) %collective-permute-start.5) | collective-permute-done | bytes 131104 | tf_op jit(solution)/shard_map/ppermute | solution.py:251
  111.2 4.2 %collective-permute-done.6 = bf16[256,256]{1,0:T(8,128)(2,1)S(1)} collective-permute-done((bf16[256,256]{1,0:T(8,128)(2,1)S(1)}, bf16[256,256]{1,0:T(8,128)(2,1)S(1)}, u32[]{:S(2)}, u32[]{:S(2)}) %collective-permute-start.6) | collective-permute-done | bytes 131104 | tf_op jit(solution)/shard_map/ppermute | solution.py:251
  115.4 2.1 collective-permute-start.27
  117.5 1.6 collective-permute-start.18
  119.1 1.7 collective-permute-start.19
  121.1 2.9 %collective-permute-start.22 = (bf16[2048,256]{1,0:T(8,128)(2,1)S(1)}, bf16[2048,256]{1,0:T(8,128)(2,1)S(1)}, u32[]{:S(2)}, u32[]{:S(2)}) collective-permute-start(bf16[2048,256]{1,0:T(8,128)(2,1)S(1)} %collective-permute-done.20.refs_5_), channel_id=1, source_target_pairs={{0,3},{1,0},{2,1},{3,2},{4,7},{5,4},{6,5},{7,6},{8,11},{9,8},{10,9... | collective-permute-start | bytes 3145736 | tf_op jit(solution)/shard_map/ppermute | solution.py:229
  124.0 1.0 copy-done.8
  125.0 6.7 %collective-permute-done.27.refs_2_ = bf16[128,2048]{1,0:T(8,128)(2,1)S(1)} collective-permute-done((bf16[128,2048]{1,0:T(8,128)(2,1)S(1)}, bf16[128,2048]{1,0:T(8,128)(2,1)S(1)}, u32[]{:S(2)}, u32[]{:S(2)}) %collective-permute-start.27) | collective-permute-done | bytes 524320 | tf_op jit(solution)/shard_map/ppermute | solution.py:229
  131.7 2.0 collective-permute-start.28
  133.8 40.8 %collective-permute-done.28.refs_3_ = bf16[128,2048]{1,0:T(8,128)(2,1)S(1)} collective-permute-done((bf16[128,2048]{1,0:T(8,128)(2,1)S(1)}, bf16[128,2048]{1,0:T(8,128)(2,1)S(1)}, u32[]{:S(2)}, u32[]{:S(2)}) %collective-permute-start.28) | collective-permute-done | bytes 524320 | tf_op jit(solution)/shard_map/ppermute | solution.py:229
  174.7 1.5 collective-permute-start.7
  176.2 1.0 copy-done.10
  177.2 1.1 collective-permute-start.8
  178.3 1.0 copy-done.12
  179.3 2.2 collective-permute-start.9
  181.4 1.0 copy-done.14
  182.4 1.3 collective-permute-start.24
  183.7 0.9 copy-done.16
  184.7 2.0 collective-permute-start.26
  186.6 1.2 copy-done.3
  187.9 1.2 copy-done.5
  189.1 1.2 copy-done.7
  190.3 1.2 copy-done.9
  191.5 1.2 copy-done.11
  192.8 1.2 copy-done.13
  194.0 1.2 copy-done.15
  195.2 1.2 copy-done.17
  196.4 6.7 %hidden_units.1.hidden_ref = bf16[4,512,256]{2,1,0:T(8,128)(2,1)S(1)} custom-call(bf16[512,2048]{1,0:T(8,128)(2,1)S(1)} %bitcast.29, bf16[2048,256]{1,0:T(8,128)(2,1)S(1)} %bitcast.33, bf16[2048,256]{1,0:T(8,128)(2,1)S(1)} %bitcast.36, bf16[2048,256]{1,0:T(8,128)(2,1)S(1)} %copy-done.7, bf16[2048,256]{1,0:T(8,128)(2,1)S(1)} %copy-done.11, ...), custom_call_target="tpu_custom_call" | custom-call | flops 4294967296 | bytes 10485760 | tf_op jit(solution)/shard_map/hidden_units/pallas_call | solution.py:142
  203.1 1.0 copy-done.1
  204.0 6.0 %down_product.2.refs_2_ = f32[512,2048]{1,0:T(8,128)} custom-call(bf16[4,512,256]{2,1,0:T(8,128)(2,1)} %copy-done.1, bf16[256,2048]{1,0:T(8,128)(2,1)} %bitcast.39, bf16[128,2048]{1,0:T(8,128)(2,1)} %collective-permute-done.23.refs_1_, bf16[128,2048]{1,0:T(8,128)(2,1)} %copy-done.20, bf16[128,2048]{1,0:T(8,128)(2,1)} %copy-done.21, ...), custom_call_target="tpu_custom_call" | custom-call | flops 1610612736 | bytes 4194304 | tf_op jit(solution)/shard_map/down_product/pallas_call | solution.py:178
  210.0 5.1 %down_product.3 = bf16[512,2048]{1,0:T(8,128)(2,1)} custom-call(bf16[4,512,256]{2,1,0:T(8,128)(2,1)} %copy-done.1, bf16[128,2048]{1,0:T(8,128)(2,1)} %collective-permute-done.24.refs_0_, bf16[128,2048]{1,0:T(8,128)(2,1)} %collective-permute-done.26.refs_1_, f32[512,2048]{1,0:T(8,128)} %down_product.2.refs_2_), custom_call_target="tpu_custom_call" | custom-call | flops 536870912 | bytes 4194304 | tf_op jit(solution)/shard_map/down_product/pallas_call | solution.py:178
  215.2 9.4 %all-to-all-start.1 = ((bf16[64,8,2048]{2,1,0:T(8,128)(2,1)}), bf16[64,8,2048]{2,1,0:T(8,128)(2,1)}, u32[]{:S(2)}, u32[]{:S(2)}) async-start(bf16[64,8,2048]{2,1,0:T(8,128)(2,1)} %bitcast.38), calls=%async_computation.1 | async-start | bytes 4194304 | tf_op jit(solution)/shard_map/all_to_all | solution.py:284
  227.4 1.5 collective-permute-done.11.refs_5_
  228.9 1.6 collective-permute-done.12.refs_6_
  230.5 1.5 collective-permute-done.13.refs_7_
  232.0 5.5 %attention.1 = bf16[256,256]{1,0:T(8,128)(2,1)S(1)} custom-call(s32[1]{0:T(128)} %bitcast.place_ref, f32[2]{0:T(128)S(1)} %copy-done.18, bf16[256,256]{1,0:T(8,128)(2,1)S(1)} %bitcast.30, f32[1,128]{1,0:T(1,128)S(1)} %bitcast.37, bf16[2048,256]{1,0:T(8,128)(2,1)S(1)} %constant_dynamic-update-slice_fusion.refs_0_, ...), custom_call_target="tpu_custom_call" | custom-call | flops 12884901888 | bytes 8388608 | tf_op jit(solution)/shard_map/attention/pallas_call | solution.py:89
  237.5 1.2 collective-permute-start.15
  238.7 1.4 collective-permute-start.14
  240.1 1.8 collective-permute-start.16
  242.0 1.1 collective-permute-done.15
  243.1 1.5 fusion.10
  244.6 1.5 fusion.12
  246.2 1.5 fusion.8
  247.7 2.2 fusion.3
  249.9 25.8 %all-to-all-done.1 = bf16[64,8,2048]{2,1,0:T(8,128)(2,1)} async-done(((bf16[64,8,2048]{2,1,0:T(8,128)(2,1)}), bf16[64,8,2048]{2,1,0:T(8,128)(2,1)}, u32[]{:S(2)}, u32[]{:S(2)}) %all-to-all-start.1) | async-done | bytes 2097184 | tf_op jit(solution)/shard_map/all_to_all | solution.py:284
  275.8 2.9 %convolution_convert_fusion.1 = bf16[128,2048]{1,0:T(8,128)(2,1)} fusion(bf16[64,8,2048]{2,1,0:T(8,128)(2,1)} %all-to-all-done.1, f32[128]{0:T(128)S(1)} %get-tuple-element.12, s32[128]{0:T(128)S(1)} %get-tuple-element.3, f32[128]{0:T(128)S(1)} %get-tuple-element.11, s32[128]{0:T(128)S(1)} %get-tuple-element.2), kind=kOutput, calls=%fused_computation.2 | convolution fusion | flops 269090816 | bytes 2623488 | tf_op jit(solution)/shard_map/dot_general | solution.py:287
  (80 shorter events, 6.2 us)
Async XLA Ops:
  0.6 0.7 copy-start
  6.5 12.2 %copy-start.23 = (bf16[256,1,128]{2,0,1:T(8,128)(2,1)S(1)}, bf16[256,1,128]{2,0,1:T(8,128)(2,1)}, u32[]{:S(2)}) copy-start(bf16[256,1,128]{2,0,1:T(8,128)(2,1)} %param.15) | copy-start | bytes 196612
  6.6 12.2 %copy-start.24 = (bf16[256,1,128]{2,0,1:T(8,128)(2,1)S(1)}, bf16[256,1,128]{2,0,1:T(8,128)(2,1)}, u32[]{:S(2)}) copy-start(bf16[256,1,128]{2,0,1:T(8,128)(2,1)} %param.14) | copy-start | bytes 196612
  6.6 180.1 %all-to-all-start = ((bf16[64,8,2048]{2,1,0:T(8,128)(2,1)}), bf16[64,8,2048]{2,1,0:T(8,128)(2,1)S(1)}, u32[]{:S(2)}, u32[]{:S(2)}) async-start(bf16[64,8,2048]{2,1,0:T(8,128)(2,1)} %fusion), calls=%async_computation | async-start | bytes 4194304 | tf_op jit(solution)/shard_map/all_to_all | solution.py:273
  18.7 98.8 %copy-start.4 = (bf16[1,2048,256]{2,1,0:T(8,128)(2,1)S(1)}, bf16[1,2048,256]{2,1,0:T(8,128)(2,1)}, u32[]{:S(2)}) copy-start(bf16[1,2048,256]{2,1,0:T(8,128)(2,1)} %param.24) | copy-start | bytes 3145732
  18.7 100.4 %copy-start.2 = (bf16[1,2048,256]{2,1,0:T(8,128)(2,1)S(1)}, bf16[1,2048,256]{2,1,0:T(8,128)(2,1)}, u32[]{:S(2)}) copy-start(bf16[1,2048,256]{2,1,0:T(8,128)(2,1)} %param.23) | copy-start | bytes 3145732
  18.8 52.3 %collective-permute-start = (bf16[256,256]{1,0:T(8,128)(2,1)S(1)}, bf16[256,256]{1,0:T(8,128)(2,1)S(1)}, u32[]{:S(2)}, u32[]{:S(2)}) collective-permute-start(bf16[256,256]{1,0:T(8,128)(2,1)S(1)} %get-tuple-element.9), channel_id=1, source_target_pairs={{0,32},{4,36},{8,40},{12,44},{16,48},{20,52},{24,56},{28,60},{32,6... | collective-permute-start | bytes 393224 | tf_op jit(solution)/shard_map/ppermute | solution.py:251
  20.3 100.4 %collective-permute-start.17 = (bf16[2048,256]{1,0:T(8,128)(2,1)}, bf16[2048,256]{1,0:T(8,128)(2,1)S(1)}, u32[]{:S(2)}, u32[]{:S(2)}) collective-permute-start(bf16[2048,256]{1,0:T(8,128)(2,1)} %bitcast.31), channel_id=1, source_target_pairs={{0,1},{1,2},{2,3},{3,0},{4,5},{5,6},{6,7},{7,4},{8,9},{9,10},{10,1... | collective-permute-start | bytes 3145736 | tf_op jit(solution)/shard_map/ppermute | solution.py:229
  21.9 99.2 %collective-permute-start.20 = (bf16[2048,256]{1,0:T(8,128)(2,1)}, bf16[2048,256]{1,0:T(8,128)(2,1)S(1)}, u32[]{:S(2)}, u32[]{:S(2)}) collective-permute-start(bf16[2048,256]{1,0:T(8,128)(2,1)} %bitcast.34), channel_id=1, source_target_pairs={{0,3},{1,0},{2,1},{3,2},{4,7},{5,4},{6,5},{7,6},{8,11},{9,8},{10,9... | collective-permute-start | bytes 3145736 | tf_op jit(solution)/shard_map/ppermute | solution.py:229
  23.6 54.6 %collective-permute-start.1 = (bf16[256,256]{1,0:T(8,128)(2,1)S(1)}, bf16[256,256]{1,0:T(8,128)(2,1)S(1)}, u32[]{:S(2)}, u32[]{:S(2)}) collective-permute-start(bf16[256,256]{1,0:T(8,128)(2,1)S(1)} %get-tuple-element.9), channel_id=1, source_target_pairs={{0,64},{4,68},{8,72},{12,76},{16,80},{20,84},{24,88},{28,92},{32,9... | collective-permute-start | bytes 393224 | tf_op jit(solution)/shard_map/ppermute | solution.py:251
  26.0 60.9 %collective-permute-start.2 = (bf16[256,256]{1,0:T(8,128)(2,1)S(1)}, bf16[256,256]{1,0:T(8,128)(2,1)S(1)}, u32[]{:S(2)}, u32[]{:S(2)}) collective-permute-start(bf16[256,256]{1,0:T(8,128)(2,1)S(1)} %get-tuple-element.9), channel_id=1, source_target_pairs={{0,96},{4,100},{8,104},{12,108},{16,112},{20,116},{24,120},{28,124... | collective-permute-start | bytes 393224 | tf_op jit(solution)/shard_map/ppermute | solution.py:251
  71.1 19.5 %collective-permute-start.3 = (bf16[256,256]{1,0:T(8,128)(2,1)S(1)}, bf16[256,256]{1,0:T(8,128)(2,1)S(1)}, u32[]{:S(2)}, u32[]{:S(2)}) collective-permute-start(bf16[256,256]{1,0:T(8,128)(2,1)S(1)} %get-tuple-element.9), channel_id=1, source_target_pairs={{0,128},{4,132},{8,136},{12,140},{16,144},{20,148},{24,152},{28,15... | collective-permute-start | bytes 393224 | tf_op jit(solution)/shard_map/ppermute | solution.py:251
  78.1 39.4 %collective-permute-start.23 = (bf16[128,2048]{1,0:T(8,128)(2,1)S(1)}, bf16[128,2048]{1,0:T(8,128)(2,1)}, u32[]{:S(2)}, u32[]{:S(2)}) collective-permute-start(bf16[128,2048]{1,0:T(8,128)(2,1)S(1)} %get-tuple-element.5), channel_id=1, source_target_pairs={{0,1},{1,2},{2,3},{3,0},{4,5},{5,6},{6,7},{7,4},{8,9},{9,10},{10,1... | collective-permute-start | bytes 1572872 | tf_op jit(solution)/shard_map/ppermute | solution.py:229
  86.9 32.2 %collective-permute-start.25 = (bf16[128,2048]{1,0:T(8,128)(2,1)S(1)}, bf16[128,2048]{1,0:T(8,128)(2,1)}, u32[]{:S(2)}, u32[]{:S(2)}) collective-permute-start(bf16[128,2048]{1,0:T(8,128)(2,1)S(1)} %get-tuple-element.4), channel_id=1, source_target_pairs={{0,3},{1,0},{2,1},{3,2},{4,7},{5,4},{6,5},{7,6},{8,11},{9,8},{10,9... | collective-permute-start | bytes 1572872 | tf_op jit(solution)/shard_map/ppermute | solution.py:229
  90.5 8.4 %collective-permute-start.4 = (bf16[256,256]{1,0:T(8,128)(2,1)S(1)}, bf16[256,256]{1,0:T(8,128)(2,1)S(1)}, u32[]{:S(2)}, u32[]{:S(2)}) collective-permute-start(bf16[256,256]{1,0:T(8,128)(2,1)S(1)} %get-tuple-element.9), channel_id=1, source_target_pairs={{0,160},{4,164},{8,168},{12,172},{16,176},{20,180},{24,184},{28,18... | collective-permute-start | bytes 393224 | tf_op jit(solution)/shard_map/ppermute | solution.py:251
  98.9 11.5 %collective-permute-start.5 = (bf16[256,256]{1,0:T(8,128)(2,1)S(1)}, bf16[256,256]{1,0:T(8,128)(2,1)S(1)}, u32[]{:S(2)}, u32[]{:S(2)}) collective-permute-start(bf16[256,256]{1,0:T(8,128)(2,1)S(1)} %get-tuple-element.9), channel_id=1, source_target_pairs={{0,192},{4,196},{8,200},{12,204},{16,208},{20,212},{24,216},{28,22... | collective-permute-start | bytes 393224 | tf_op jit(solution)/shard_map/ppermute | solution.py:251
  110.4 5.0 %collective-permute-start.6 = (bf16[256,256]{1,0:T(8,128)(2,1)S(1)}, bf16[256,256]{1,0:T(8,128)(2,1)S(1)}, u32[]{:S(2)}, u32[]{:S(2)}) collective-permute-start(bf16[256,256]{1,0:T(8,128)(2,1)S(1)} %get-tuple-element.9), channel_id=1, source_target_pairs={{0,224},{4,228},{8,232},{12,236},{16,240},{20,244},{24,248},{28,25... | collective-permute-start | bytes 393224 | tf_op jit(solution)/shard_map/ppermute | solution.py:251
  115.4 16.3 %collective-permute-start.27 = (bf16[128,2048]{1,0:T(8,128)(2,1)S(1)}, bf16[128,2048]{1,0:T(8,128)(2,1)S(1)}, u32[]{:S(2)}, u32[]{:S(2)}) collective-permute-start(bf16[128,2048]{1,0:T(8,128)(2,1)S(1)} %get-tuple-element.4), channel_id=1, source_target_pairs={{0,1},{1,2},{2,3},{3,0},{4,5},{5,6},{6,7},{7,4},{8,9},{9,10},{10,1... | collective-permute-start | bytes 1572872 | tf_op jit(solution)/shard_map/ppermute | solution.py:229
  117.5 58.6 %collective-permute-start.18 = (bf16[2048,256]{1,0:T(8,128)(2,1)S(1)}, bf16[2048,256]{1,0:T(8,128)(2,1)S(1)}, u32[]{:S(2)}, u32[]{:S(2)}) collective-permute-start(bf16[2048,256]{1,0:T(8,128)(2,1)S(1)} %bitcast.35), channel_id=1, source_target_pairs={{0,1},{1,2},{2,3},{3,0},{4,5},{5,6},{6,7},{7,4},{8,9},{9,10},{10,1... | collective-permute-start | bytes 3145736 | tf_op jit(solution)/shard_map/ppermute | solution.py:229
  119.1 59.2 %collective-permute-start.19 = (bf16[2048,256]{1,0:T(8,128)(2,1)S(1)}, bf16[2048,256]{1,0:T(8,128)(2,1)S(1)}, u32[]{:S(2)}, u32[]{:S(2)}) collective-permute-start(bf16[2048,256]{1,0:T(8,128)(2,1)S(1)} %bitcast.32), channel_id=1, source_target_pairs={{0,3},{1,0},{2,1},{3,2},{4,7},{5,4},{6,5},{7,6},{8,11},{9,8},{10,9... | collective-permute-start | bytes 3145736 | tf_op jit(solution)/shard_map/ppermute | solution.py:229
  120.8 62.9 %copy-start.6 = (bf16[2048,256]{1,0:T(8,128)(2,1)}, bf16[2048,256]{1,0:T(8,128)(2,1)S(1)}, u32[]{:S(2)}) copy-start(bf16[2048,256]{1,0:T(8,128)(2,1)S(1)} %collective-permute-done.17.refs_2_) | copy-start | bytes 3145732
  120.8 60.7 %collective-permute-start.21 = (bf16[2048,256]{1,0:T(8,128)(2,1)S(1)}, bf16[2048,256]{1,0:T(8,128)(2,1)S(1)}, u32[]{:S(2)}, u32[]{:S(2)}) collective-permute-start(bf16[2048,256]{1,0:T(8,128)(2,1)S(1)} %collective-permute-done.17.refs_2_), channel_id=1, source_target_pairs={{0,1},{1,2},{2,3},{3,0},{4,5},{5,6},{6,7},{7,4},{8,9},{9,10},{10,1... | collective-permute-start | bytes 3145736 | tf_op jit(solution)/shard_map/ppermute | solution.py:229
  121.1 62.6 %collective-permute-start.22 = (bf16[2048,256]{1,0:T(8,128)(2,1)S(1)}, bf16[2048,256]{1,0:T(8,128)(2,1)S(1)}, u32[]{:S(2)}, u32[]{:S(2)}) collective-permute-start(bf16[2048,256]{1,0:T(8,128)(2,1)S(1)} %collective-permute-done.20.refs_5_), channel_id=1, source_target_pairs={{0,3},{1,0},{2,1},{3,2},{4,7},{5,4},{6,5},{7,6},{8,11},{9,8},{10,9... | collective-permute-start | bytes 3145736 | tf_op jit(solution)/shard_map/ppermute | solution.py:229
  124.0 1.0 copy-start.8
  131.7 52.0 %copy-start.20 = (bf16[128,2048]{1,0:T(8,128)(2,1)}, bf16[128,2048]{1,0:T(8,128)(2,1)S(1)}, u32[]{:S(2)}) copy-start(bf16[128,2048]{1,0:T(8,128)(2,1)S(1)} %collective-permute-done.27.refs_2_) | copy-start | bytes 1572868
  131.7 43.0 %collective-permute-start.28 = (bf16[128,2048]{1,0:T(8,128)(2,1)S(1)}, bf16[128,2048]{1,0:T(8,128)(2,1)S(1)}, u32[]{:S(2)}, u32[]{:S(2)}) collective-permute-start(bf16[128,2048]{1,0:T(8,128)(2,1)S(1)} %get-tuple-element.5), channel_id=1, source_target_pairs={{0,3},{1,0},{2,1},{3,2},{4,7},{5,4},{6,5},{7,6},{8,11},{9,8},{10,9... | collective-permute-start | bytes 1572872 | tf_op jit(solution)/shard_map/ppermute | solution.py:229
  174.7 9.0 %copy-start.21 = (bf16[128,2048]{1,0:T(8,128)(2,1)}, bf16[128,2048]{1,0:T(8,128)(2,1)S(1)}, u32[]{:S(2)}) copy-start(bf16[128,2048]{1,0:T(8,128)(2,1)S(1)} %collective-permute-done.28.refs_3_) | copy-start | bytes 1572868
  174.7 50.1 %collective-permute-start.7 = (bf16[2048,256]{1,0:T(8,128)(2,1)S(1)}, bf16[2048,256]{1,0:T(8,128)(2,1)}, u32[]{:S(2)}, u32[]{:S(2)}) collective-permute-start(bf16[2048,256]{1,0:T(8,128)(2,1)S(1)} %constant_dynamic-update-slice_fusion.refs_0_), channel_id=1, source_target_pairs={{0,8},{4,12},{8,16},{12,20},{16,24},{20,28},{24,0},{28,4},{32,40},... | collective-permute-start | bytes 3145736 | tf_op jit(solution)/shard_map/ppermute | solution.py:251
  176.2 1.0 copy-start.10
  177.2 48.0 %collective-permute-start.8 = (bf16[2048,256]{1,0:T(8,128)(2,1)S(1)}, bf16[2048,256]{1,0:T(8,128)(2,1)}, u32[]{:S(2)}, u32[]{:S(2)}) collective-permute-start(bf16[2048,256]{1,0:T(8,128)(2,1)S(1)} %constant_dynamic-update-slice_fusion.refs_0_), channel_id=1, source_target_pairs={{0,16},{4,20},{8,24},{12,28},{16,0},{20,4},{24,8},{28,12},{32,48},... | collective-permute-start | bytes 3145736 | tf_op jit(solution)/shard_map/ppermute | solution.py:251
  178.3 1.0 copy-start.12
  179.3 46.1 %collective-permute-start.9 = (bf16[2048,256]{1,0:T(8,128)(2,1)S(1)}, bf16[2048,256]{1,0:T(8,128)(2,1)}, u32[]{:S(2)}, u32[]{:S(2)}) collective-permute-start(bf16[2048,256]{1,0:T(8,128)(2,1)S(1)} %constant_dynamic-update-slice_fusion.refs_0_), channel_id=1, source_target_pairs={{0,24},{4,28},{8,0},{12,4},{16,8},{20,12},{24,16},{28,20},{32,56},... | collective-permute-start | bytes 3145736 | tf_op jit(solution)/shard_map/ppermute | solution.py:251
  181.4 1.0 copy-start.14
  182.4 27.6 %collective-permute-start.24 = (bf16[128,2048]{1,0:T(8,128)(2,1)}, bf16[128,2048]{1,0:T(8,128)(2,1)}, u32[]{:S(2)}, u32[]{:S(2)}) collective-permute-start(bf16[128,2048]{1,0:T(8,128)(2,1)} %collective-permute-done.23.refs_1_), channel_id=1, source_target_pairs={{0,1},{1,2},{2,3},{3,0},{4,5},{5,6},{6,7},{7,4},{8,9},{9,10},{10,1... | collective-permute-start | bytes 1572872 | tf_op jit(solution)/shard_map/ppermute | solution.py:229
  183.7 1.0 copy-start.16
  184.7 25.4 %collective-permute-start.26 = (bf16[128,2048]{1,0:T(8,128)(2,1)}, bf16[128,2048]{1,0:T(8,128)(2,1)}, u32[]{:S(2)}, u32[]{:S(2)}) collective-permute-start(bf16[128,2048]{1,0:T(8,128)(2,1)} %collective-permute-done.25.refs_4_), channel_id=1, source_target_pairs={{0,3},{1,0},{2,1},{3,2},{4,7},{5,4},{6,5},{7,6},{8,11},{9,8},{10,9... | collective-permute-start | bytes 1572872 | tf_op jit(solution)/shard_map/ppermute | solution.py:229
  186.6 1.2 copy-start.3
  187.8 1.2 copy-start.5
  189.1 1.2 copy-start.7
  190.3 1.2 copy-start.9
  191.5 1.2 copy-start.11
  192.8 1.2 copy-start.13
  194.0 1.2 copy-start.15
  195.2 1.2 copy-start.17
  203.1 1.0 copy-start.1
  215.2 10.5 %copy-start.22 = (bf16[256,2,128]{2,1,0:T(2,128)(2,1)S(1)}, bf16[256,2,128]{2,1,0:T(2,128)(2,1)}, u32[]{:S(2)}) copy-start(bf16[256,2,128]{2,1,0:T(2,128)(2,1)} %param.13) | copy-start | bytes 393220
  215.2 16.8 %copy-start.18 = (f32[2]{0:T(128)S(1)}, f32[2]{0:T(128)}, u32[]{:S(2)}) copy-start(f32[2]{0:T(128)} %lam_ref.1) | copy-start | bytes 28
  215.2 16.8 %copy-start.19 = (f32[128]{0:T(128)S(1)}, f32[128]{0:T(128)}, u32[]{:S(2)}) copy-start(f32[128]{0:T(128)} %param.17) | copy-start | bytes 1540
  215.2 60.6 %all-to-all-start.1 = ((bf16[64,8,2048]{2,1,0:T(8,128)(2,1)}), bf16[64,8,2048]{2,1,0:T(8,128)(2,1)}, u32[]{:S(2)}, u32[]{:S(2)}) async-start(bf16[64,8,2048]{2,1,0:T(8,128)(2,1)} %bitcast.38), calls=%async_computation.1 | async-start | bytes 4194304 | tf_op jit(solution)/shard_map/all_to_all | solution.py:284
  224.6 2.7 collective-permute-start.10
  224.8 4.0 %collective-permute-start.11 = (bf16[2048,256]{1,0:T(8,128)(2,1)}, bf16[2048,256]{1,0:T(8,128)(2,1)S(1)}, u32[]{:S(2)}, u32[]{:S(2)}) collective-permute-start(bf16[2048,256]{1,0:T(8,128)(2,1)} %collective-permute-done.7.refs_1_), channel_id=1, source_target_pairs={{0,4},{4,0},{8,12},{12,8},{16,20},{20,16},{24,28},{28,24},{32,36},... | collective-permute-start | bytes 3145736 | tf_op jit(solution)/shard_map/ppermute | solution.py:251
  225.2 5.3 %collective-permute-start.12 = (bf16[2048,256]{1,0:T(8,128)(2,1)}, bf16[2048,256]{1,0:T(8,128)(2,1)}, u32[]{:S(2)}, u32[]{:S(2)}) collective-permute-start(bf16[2048,256]{1,0:T(8,128)(2,1)} %collective-permute-done.8.refs_2_), channel_id=1, source_target_pairs={{0,4},{4,0},{8,12},{12,8},{16,20},{20,16},{24,28},{28,24},{32,36},... | collective-permute-start | bytes 3145736 | tf_op jit(solution)/shard_map/ppermute | solution.py:251
  225.3 6.7 %collective-permute-start.13 = (bf16[2048,256]{1,0:T(8,128)(2,1)}, bf16[2048,256]{1,0:T(8,128)(2,1)}, u32[]{:S(2)}, u32[]{:S(2)}) collective-permute-start(bf16[2048,256]{1,0:T(8,128)(2,1)} %collective-permute-done.9.refs_3_), channel_id=1, source_target_pairs={{0,4},{4,0},{8,12},{12,8},{16,20},{20,16},{24,28},{28,24},{32,36},... | collective-permute-start | bytes 3145736 | tf_op jit(solution)/shard_map/ppermute | solution.py:251
  237.5 5.6 %collective-permute-start.15 = (bf16[64,256]{1,0:T(8,128)(2,1)S(1)}, bf16[64,256]{1,0:T(8,128)(2,1)S(1)}, u32[]{:S(2)}, u32[]{:S(2)}) collective-permute-start(bf16[64,256]{1,0:T(8,128)(2,1)S(1)} %get-tuple-element.8), channel_id=1, source_target_pairs={{0,2},{1,3},{2,0},{3,1},{4,6},{5,7},{6,4},{7,5},{8,10},{9,11},{10,... | collective-permute-start | bytes 98312 | tf_op jit(solution)/shard_map/ppermute | solution.py:229
  238.7 5.9 %collective-permute-start.14 = (bf16[64,256]{1,0:T(8,128)(2,1)S(1)}, bf16[64,256]{1,0:T(8,128)(2,1)S(1)}, u32[]{:S(2)}, u32[]{:S(2)}) collective-permute-start(bf16[64,256]{1,0:T(8,128)(2,1)S(1)} %get-tuple-element.6), channel_id=1, source_target_pairs={{0,1},{1,2},{2,3},{3,0},{4,5},{5,6},{6,7},{7,4},{8,9},{9,10},{10,1... | collective-permute-start | bytes 98312 | tf_op jit(solution)/shard_map/ppermute | solution.py:229
  240.1 6.0 %collective-permute-start.16 = (bf16[64,256]{1,0:T(8,128)(2,1)S(1)}, bf16[64,256]{1,0:T(8,128)(2,1)S(1)}, u32[]{:S(2)}, u32[]{:S(2)}) collective-permute-start(bf16[64,256]{1,0:T(8,128)(2,1)S(1)} %get-tuple-element.7), channel_id=1, source_target_pairs={{0,3},{1,0},{2,1},{3,2},{4,7},{5,4},{6,5},{7,6},{8,11},{9,8},{10,9... | collective-permute-start | bytes 98312 | tf_op jit(solution)/shard_map/ppermute | solution.py:229

commit v3 on v2

--- a/solution.py
+++ b/solution.py
@@ -10,6 +10,7 @@
 
 EPSILON = 1e-06
 MASKED = -1e30
+WHOLE_VMEM = 60 * 1024 * 1024
 EP_SIZES = (8, 4, 2)
 
 
@@ -115,23 +116,19 @@
     out_ref, rows_ref, weights_ref, rows_sem, sems = refs[2 * shards :]
     rows_copy = pltpu.make_async_copy(rows_hbm, rows_ref, rows_sem)
     rows_copy.start()
-    copies = [pltpu.make_async_copy(weight_refs[i], weights_ref.at[i], sems.at[i]) for i in range(2 * shards)]
-    for copy in copies:
-        copy.start()
-    count = rows_ref.shape[0]
-    block = count // 2
+    for i in range(2 * shards):
+        pltpu.make_async_copy(weight_refs[i], weights_ref.at[i], sems.at[i]).start()
     rows_copy.wait()
-    for shard in range(shards):
-        copies[2 * shard].wait()
-        copies[2 * shard + 1].wait()
-
-        @pl.loop(0, count // block)
-        def _(step):
-            start = pl.multiple_of(step * block, block)
-            rows = rows_ref[pl.ds(start, block), :]
-            gate_out = jnp.dot(rows, weights_ref[2 * shard], preferred_element_type=jnp.float32)
-            up_out = jnp.dot(rows, weights_ref[2 * shard + 1], preferred_element_type=jnp.float32)
-            out_ref[shard, pl.ds(start, block), :] = (jax.nn.silu(gate_out) * up_out).astype(jnp.bfloat16)
+
+    @pl.loop(0, shards)
+    def _(shard):
+        for i in range(2):
+            at = 2 * shard + i
+            pltpu.make_async_copy(weight_refs[i], weights_ref.at[at], sems.at[at]).wait()
+        rows = rows_ref[...]
+        gate_out = jnp.dot(rows, weights_ref[2 * shard], preferred_element_type=jnp.float32)
+        up_out = jnp.dot(rows, weights_ref[2 * shard + 1], preferred_element_type=jnp.float32)
+        out_ref[shard] = (jax.nn.silu(gate_out) * up_out).astype(jnp.bfloat16)
 
 
 def hidden_units(rows, weights):
@@ -155,7 +152,7 @@
             bytes_accessed=2 * depth * (count + 2 * units * shards),
             transcendentals=count * units * shards,
         ),
-        compiler_params=pltpu.CompilerParams(vmem_limit_bytes=32 * 1024 * 1024),
+        compiler_params=pltpu.CompilerParams(vmem_limit_bytes=WHOLE_VMEM),
         name="hidden_units",
     )(rows, *flat)
 
@@ -186,6 +183,7 @@
         cost_estimate=pl.CostEstimate(
             flops=2 * rows * width * depth, bytes_accessed=4 * rows * width, transcendentals=0
         ),
+        compiler_params=pltpu.CompilerParams(vmem_limit_bytes=WHOLE_VMEM),
         name="down_product",
     )(hidden, *weights, *begun)
 

time: 280 us -> 276 us (0.986)
  the two profiles are of different devices: /device:TPU:2 before, /device:TPU:230 now
where the time goes in v3:
time: 276 us; the launch traced here: 275 us
  waiting for transfers between devices  134 us (49%)
  starting transfers between devices  69 us (25%)
  Pallas kernels  53.8 us (19%)
  matrix products  12.9 us (5%)
  local copies, waits for them, and re-layouts  3.18 us (1%)
    ppermute x14, waiting for transfers between devices, spread(): return lax.ppermute(x, 'ep', ep_shift(*shift))  84.3 us
    ppermute x15, waiting for transfers between devices, send(): return lax.ppermute(x, 'tp', way)  49.4 us
    pallas_call x1, Pallas kernels, attention(): pl.pallas_call(functools.partial(attention_body, heads=heads, dim=width /...  32.7 us
    ppermute x15, starting transfers between devices, send(): return lax.ppermute(x, 'tp', way)  30 us
    ppermute x14, starting transfers between devices, spread(): return lax.ppermute(x, 'ep', ep_shift(*shift))  18.7 us
    pallas_call x2, Pallas kernels, down_product(): pl.pallas_call(functools.partial(down_body, parts=len(weights), begun=len...  11.2 us
    all_to_all x1, starting transfers between devices, local(): lax.all_to_all(out.reshape(experts, capacity, -1), 'ep', split_axis=0, co...  10.9 us
    pallas_call x1, Pallas kernels, hidden_units(): pl.pallas_call(functools.partial(hidden_body, shards=shards), out_shape=j...  9.95 us
  transfers between devices with their start and end apart: 31, of which 11 were waited for; matrix products, arithmetic and copies ran while one was open for 3% of the time, Pallas kernels for 20%

profile of v3, /device:TPU:230, one launch (start us, length us, event | category | flops | bytes accessed | tf_op | source)
XLA Modules:
  0.0 275.1 jit_solution(3183694733064924526)
XLA Ops:
  0.6 0.0 copy-start
  0.7 0.7 copy-done
  1.3 0.1 copy.18
  1.4 0.1 eq.81
  1.6 0.2 convert_reduce_fusion
  1.8 0.1 reduce_sum.21
  1.9 0.2 slice_reduce_fusion.1
  2.1 1.2 fusion.5
  3.4 3.2 %fusion = bf16[64,8,2048]{2,1,0:T(8,128)(2,1)} fusion(f32[2048]{0:T(1024)} %param.20, f32[128]{0:T(128)S(1)} %add_rsqrt_fusion, bf16[512,2048]{1,0:T(8,128)(2,1)} %param.19, s32[]{:T(128)S(6)} %select_n.77, s32[128]{0:T(128)S(1)} %get-tuple-element.3, s32[128]{0:T(128)S(1)} %get-tuple-element.2), kind=kOutput, calls=%fused_computation.1 | convolution fusion | flops 270729216 | bytes 2631172 | tf_op jit(solution)/shard_map/dot_general | solution.py:270
  6.6 9.4 %all-to-all-start = ((bf16[64,8,2048]{2,1,0:T(8,128)(2,1)}), bf16[64,8,2048]{2,1,0:T(8,128)(2,1)}, u32[]{:S(2)}, u32[]{:S(2)}) async-start(bf16[64,8,2048]{2,1,0:T(8,128)(2,1)} %fusion), calls=%async_computation | async-start | bytes 4194304 | tf_op jit(solution)/shard_map/all_to_all | solution.py:271
  16.0 0.3 collective-permute-start
  16.4 1.6 collective-permute-start.17
  18.0 1.7 collective-permute-start.20
  19.6 2.4 collective-permute-start.1
  22.0 3.7 %collective-permute-start.2 = (bf16[256,256]{1,0:T(8,128)(2,1)S(1)}, bf16[256,256]{1,0:T(8,128)(2,1)S(1)}, u32[]{:S(2)}, u32[]{:S(2)}) collective-permute-start(bf16[256,256]{1,0:T(8,128)(2,1)S(1)} %get-tuple-element.9), channel_id=1, source_target_pairs={{0,96},{4,100},{8,104},{12,108},{16,112},{20,116},{24,120},{28,124... | collective-permute-start | bytes 393224 | tf_op jit(solution)/shard_map/ppermute | solution.py:249
  25.7 40.9 %collective-permute-done = bf16[256,256]{1,0:T(8,128)(2,1)S(1)} collective-permute-done((bf16[256,256]{1,0:T(8,128)(2,1)S(1)}, bf16[256,256]{1,0:T(8,128)(2,1)S(1)}, u32[]{:S(2)}, u32[]{:S(2)}) %collective-permute-start) | collective-permute-done | bytes 131104 | tf_op jit(solution)/shard_map/ppermute | solution.py:249
  66.6 2.0 collective-permute-start.3
  68.6 0.1 slice_bitcast_fusion
  68.7 3.8 %collective-permute-done.1 = bf16[256,256]{1,0:T(8,128)(2,1)S(1)} collective-permute-done((bf16[256,256]{1,0:T(8,128)(2,1)S(1)}, bf16[256,256]{1,0:T(8,128)(2,1)S(1)}, u32[]{:S(2)}, u32[]{:S(2)}) %collective-permute-start.1) | collective-permute-done | bytes 131104 | tf_op jit(solution)/shard_map/ppermute | solution.py:249
  72.5 1.6 collective-permute-start.23
  74.0 6.4 %collective-permute-done.2 = bf16[256,256]{1,0:T(8,128)(2,1)S(1)} collective-permute-done((bf16[256,256]{1,0:T(8,128)(2,1)S(1)}, bf16[256,256]{1,0:T(8,128)(2,1)S(1)}, u32[]{:S(2)}, u32[]{:S(2)}) %collective-permute-start.2) | collective-permute-done | bytes 131104 | tf_op jit(solution)/shard_map/ppermute | solution.py:249
  80.5 3.0 %collective-permute-start.25 = (bf16[128,2048]{1,0:T(8,128)(2,1)S(1)}, bf16[128,2048]{1,0:T(8,128)(2,1)}, u32[]{:S(2)}, u32[]{:S(2)}) collective-permute-start(bf16[128,2048]{1,0:T(8,128)(2,1)S(1)} %get-tuple-element.4), channel_id=1, source_target_pairs={{0,3},{1,0},{2,1},{3,2},{4,7},{5,4},{6,5},{7,6},{8,11},{9,8},{10,9... | collective-permute-start | bytes 1572872 | tf_op jit(solution)/shard_map/ppermute | solution.py:227
  83.5 0.0 collective-permute-done.3
  83.5 2.2 collective-permute-start.4
  85.7 10.9 %collective-permute-done.4 = bf16[256,256]{1,0:T(8,128)(2,1)S(1)} collective-permute-done((bf16[256,256]{1,0:T(8,128)(2,1)S(1)}, bf16[256,256]{1,0:T(8,128)(2,1)S(1)}, u32[]{:S(2)}, u32[]{:S(2)}) %collective-permute-start.4) | collective-permute-done | bytes 131104 | tf_op jit(solution)/shard_map/ppermute | solution.py:249
  96.6 0.0 collective-permute-start.5
  96.6 8.7 %collective-permute-done.5 = bf16[256,256]{1,0:T(8,128)(2,1)S(1)} collective-permute-done((bf16[256,256]{1,0:T(8,128)(2,1)S(1)}, bf16[256,256]{1,0:T(8,128)(2,1)S(1)}, u32[]{:S(2)}, u32[]{:S(2)}) %collective-permute-start.5) | collective-permute-done | bytes 131104 | tf_op jit(solution)/shard_map/ppermute | solution.py:249
  105.4 4.4 %collective-permute-start.6 = (bf16[256,256]{1,0:T(8,128)(2,1)S(1)}, bf16[256,256]{1,0:T(8,128)(2,1)S(1)}, u32[]{:S(2)}, u32[]{:S(2)}) collective-permute-start(bf16[256,256]{1,0:T(8,128)(2,1)S(1)} %get-tuple-element.9), channel_id=1, source_target_pairs={{0,224},{4,228},{8,232},{12,236},{16,240},{20,244},{24,248},{28,25... | collective-permute-start | bytes 393224 | tf_op jit(solution)/shard_map/ppermute | solution.py:249
  109.7 2.5 collective-permute-done.6
  112.3 2.1 collective-permute-start.27
  114.4 1.6 collective-permute-start.18
  116.0 0.0 collective-permute-done.25.refs_4_
  116.0 1.7 collective-permute-start.19
  117.6 0.4 collective-permute-start.21
  118.0 2.9 %collective-permute-start.22 = (bf16[2048,256]{1,0:T(8,128)(2,1)S(1)}, bf16[2048,256]{1,0:T(8,128)(2,1)S(1)}, u32[]{:S(2)}, u32[]{:S(2)}) collective-permute-start(bf16[2048,256]{1,0:T(8,128)(2,1)S(1)} %collective-permute-done.20.refs_5_), channel_id=1, source_target_pairs={{0,3},{1,0},{2,1},{3,2},{4,7},{5,4},{6,5},{7,6},{8,11},{9,8},{10,9... | collective-permute-start | bytes 3145736 | tf_op jit(solution)/shard_map/ppermute | solution.py:227
  120.9 7.7 %collective-permute-done.27.refs_2_ = bf16[128,2048]{1,0:T(8,128)(2,1)S(1)} collective-permute-done((bf16[128,2048]{1,0:T(8,128)(2,1)S(1)}, bf16[128,2048]{1,0:T(8,128)(2,1)S(1)}, u32[]{:S(2)}, u32[]{:S(2)}) %collective-permute-start.27) | collective-permute-done | bytes 524320 | tf_op jit(solution)/shard_map/ppermute | solution.py:227
  128.6 2.0 collective-permute-start.28
  130.7 41.3 %collective-permute-done.28.refs_3_ = bf16[128,2048]{1,0:T(8,128)(2,1)S(1)} collective-permute-done((bf16[128,2048]{1,0:T(8,128)(2,1)S(1)}, bf16[128,2048]{1,0:T(8,128)(2,1)S(1)}, u32[]{:S(2)}, u32[]{:S(2)}) %collective-permute-start.28) | collective-permute-done | bytes 524320 | tf_op jit(solution)/shard_map/ppermute | solution.py:227
  172.1 0.4 collective-permute-start.7
  172.5 2.4 collective-permute-start.8
  175.0 0.1 collective-permute-start.9
  175.1 1.4 collective-permute-start.24
  176.5 1.0 copy-done.15
  177.5 2.8 %collective-permute-start.26 = (bf16[128,2048]{1,0:T(8,128)(2,1)}, bf16[128,2048]{1,0:T(8,128)(2,1)}, u32[]{:S(2)}, u32[]{:S(2)}) collective-permute-start(bf16[128,2048]{1,0:T(8,128)(2,1)} %collective-permute-done.25.refs_4_), channel_id=1, source_target_pairs={{0,3},{1,0},{2,1},{3,2},{4,7},{5,4},{6,5},{7,6},{8,11},{9,8},{10,9... | collective-permute-start | bytes 1572872 | tf_op jit(solution)/shard_map/ppermute | solution.py:227
  180.2 10.0 %hidden_units.1.hidden_ref = bf16[4,512,256]{2,1,0:T(8,128)(2,1)} custom-call(bf16[512,2048]{1,0:T(8,128)(2,1)} %bitcast.7.rows_hbm, bf16[2048,256]{1,0:T(8,128)(2,1)} %bitcast.8.refs_0_, bf16[2048,256]{1,0:T(8,128)(2,1)} %bitcast.36, bf16[2048,256]{1,0:T(8,128)(2,1)} %copy-done.10, bf16[2048,256]{1,0:T(8,128)(2,1)} %copy-done.12, ...), custom_call_target="tpu_custom_call" | custom-call | flops 4294967296 | bytes 10485760 | tf_op jit(solution)/shard_map/hidden_units/pallas_call | solution.py:139
  190.2 6.0 %down_product.2.refs_2_ = f32[512,2048]{1,0:T(8,128)} custom-call(bf16[4,512,256]{2,1,0:T(8,128)(2,1)} %hidden_units.1.hidden_ref, bf16[256,2048]{1,0:T(8,128)(2,1)} %bitcast.32, bf16[128,2048]{1,0:T(8,128)(2,1)} %collective-permute-done.23.refs_1_, bf16[128,2048]{1,0:T(8,128)(2,1)} %copy-done.4, bf16[128,2048]{1,0:T(8,128)(2,1)} %copy-done.5, ...), custom_call_target="tpu_custom_call" | custom-call | flops 1610612736 | bytes 4194304 | tf_op jit(solution)/shard_map/down_product/pallas_call | solution.py:175
  196.2 5.2 %down_product.3 = bf16[512,2048]{1,0:T(8,128)(2,1)} custom-call(bf16[4,512,256]{2,1,0:T(8,128)(2,1)} %hidden_units.1.hidden_ref, bf16[128,2048]{1,0:T(8,128)(2,1)} %collective-permute-done.24.refs_0_, bf16[128,2048]{1,0:T(8,128)(2,1)} %collective-permute-done.26.refs_1_, f32[512,2048]{1,0:T(8,128)} %down_product.2.refs_2_), custom_call_target="tpu_custom_call" | custom-call | flops 536870912 | bytes 4194304 | tf_op jit(solution)/shard_map/down_product/pallas_call | solution.py:175
  201.4 10.9 %all-to-all-start.1 = ((bf16[64,8,2048]{2,1,0:T(8,128)(2,1)}), bf16[64,8,2048]{2,1,0:T(8,128)(2,1)}, u32[]{:S(2)}, u32[]{:S(2)}) async-start(bf16[64,8,2048]{2,1,0:T(8,128)(2,1)} %bitcast.31), calls=%async_computation.1 | async-start | bytes 4194304 | tf_op jit(solution)/shard_map/all_to_all | solution.py:282
  212.3 0.2 collective-permute-start.10
  212.5 0.4 collective-permute-start.11
  212.9 0.1 collective-permute-start.12
  213.0 8.8 %collective-permute-done.9.refs_3_ = bf16[2048,256]{1,0:T(8,128)(2,1)} collective-permute-done((bf16[2048,256]{1,0:T(8,128)(2,1)S(1)}, bf16[2048,256]{1,0:T(8,128)(2,1)}, u32[]{:S(2)}, u32[]{:S(2)}) %collective-permute-start.9) | collective-permute-done | bytes 1048608 | tf_op jit(solution)/shard_map/ppermute | solution.py:249
  221.9 0.7 constant_dynamic-slice_fusion
  222.6 2.3 collective-permute-done.13.refs_7_
  224.9 32.7 %attention.1 = bf16[256,256]{1,0:T(8,128)(2,1)S(1)} custom-call(s32[1]{0:T(128)} %bitcast.place_ref, f32[2]{0:T(128)S(1)} %copy-done.1, bf16[256,256]{1,0:T(8,128)(2,1)S(1)} %bitcast.29, f32[1,128]{1,0:T(1,128)S(1)} %bitcast.30, bf16[2048,256]{1,0:T(8,128)(2,1)S(1)} %constant_dynamic-update-slice_fusion.refs_0_, ...), custom_call_target="tpu_custom_call" | custom-call | flops 12884901888 | bytes 8388608 | tf_op jit(solution)/shard_map/attention/pallas_call | solution.py:90
  257.6 4.1 %collective-permute-start.15 = (bf16[64,256]{1,0:T(8,128)(2,1)S(1)}, bf16[64,256]{1,0:T(8,128)(2,1)S(1)}, u32[]{:S(2)}, u32[]{:S(2)}) collective-permute-start(bf16[64,256]{1,0:T(8,128)(2,1)S(1)} %get-tuple-element.8), channel_id=1, source_target_pairs={{0,2},{1,3},{2,0},{3,1},{4,6},{5,7},{6,4},{7,5},{8,10},{9,11},{10,... | collective-permute-start | bytes 98312 | tf_op jit(solution)/shard_map/ppermute | solution.py:227
  261.7 1.9 collective-permute-start.14
  263.6 1.4 collective-permute-start.16
  265.0 1.5 fusion.10
  266.5 0.4 collective-permute-done.14
  266.9 1.5 fusion.12
  268.4 1.5 fusion.8
  269.9 2.2 fusion.3
  272.2 2.9 %convolution_convert_fusion.1 = bf16[128,2048]{1,0:T(8,128)(2,1)} fusion(bf16[64,8,2048]{2,1,0:T(8,128)(2,1)} %all-to-all-done.1, f32[128]{0:T(128)S(1)} %get-tuple-element.12, s32[128]{0:T(128)S(1)} %get-tuple-element.3, f32[128]{0:T(128)S(1)} %get-tuple-element.11, s32[128]{0:T(128)S(1)} %get-tuple-element.2), kind=kOutput, calls=%fused_computation.2 | convolution fusion | flops 269090816 | bytes 2623488 | tf_op jit(solution)/shard_map/dot_general | solution.py:285
  (62 shorter events, 0.3 us)
Async XLA Ops:
  0.6 0.7 copy-start
  6.6 9.4 %copy-start.7 = (bf16[256,1,128]{2,0,1:T(8,128)(2,1)S(1)}, bf16[256,1,128]{2,0,1:T(8,128)(2,1)}, u32[]{:S(2)}) copy-start(bf16[256,1,128]{2,0,1:T(8,128)(2,1)} %param.15) | copy-start | bytes 196612
  6.6 9.4 %copy-start.8 = (bf16[256,1,128]{2,0,1:T(8,128)(2,1)S(1)}, bf16[256,1,128]{2,0,1:T(8,128)(2,1)}, u32[]{:S(2)}) copy-start(bf16[256,1,128]{2,0,1:T(8,128)(2,1)} %param.14) | copy-start | bytes 196612
  6.6 11.4 %copy-start.9 = (bf16[1,2048,256]{2,1,0:T(8,128)(2,1)S(1)}, bf16[1,2048,256]{2,1,0:T(8,128)(2,1)}, u32[]{:S(2)}) copy-start(bf16[1,2048,256]{2,1,0:T(8,128)(2,1)} %param.24) | copy-start | bytes 3145732
  6.6 62.0 %copy-start.3 = (bf16[1,256,2048]{2,1,0:T(8,128)(2,1)S(1)}, bf16[1,256,2048]{2,1,0:T(8,128)(2,1)}, u32[]{:S(2)}) copy-start(bf16[1,256,2048]{2,1,0:T(8,128)(2,1)} %param.25) | copy-start | bytes 3145732
  6.6 173.7 %all-to-all-start = ((bf16[64,8,2048]{2,1,0:T(8,128)(2,1)}), bf16[64,8,2048]{2,1,0:T(8,128)(2,1)}, u32[]{:S(2)}, u32[]{:S(2)}) async-start(bf16[64,8,2048]{2,1,0:T(8,128)(2,1)} %fusion), calls=%async_computation | async-start | bytes 4194304 | tf_op jit(solution)/shard_map/all_to_all | solution.py:271
  16.0 50.6 %collective-permute-start = (bf16[256,256]{1,0:T(8,128)(2,1)S(1)}, bf16[256,256]{1,0:T(8,128)(2,1)S(1)}, u32[]{:S(2)}, u32[]{:S(2)}) collective-permute-start(bf16[256,256]{1,0:T(8,128)(2,1)S(1)} %get-tuple-element.9), channel_id=1, source_target_pairs={{0,32},{4,36},{8,40},{12,44},{16,48},{20,52},{24,56},{28,60},{32,6... | collective-permute-start | bytes 393224 | tf_op jit(solution)/shard_map/ppermute | solution.py:249
  16.4 101.3 %collective-permute-start.17 = (bf16[2048,256]{1,0:T(8,128)(2,1)}, bf16[2048,256]{1,0:T(8,128)(2,1)S(1)}, u32[]{:S(2)}, u32[]{:S(2)}) collective-permute-start(bf16[2048,256]{1,0:T(8,128)(2,1)} %bitcast.8.refs_0_), channel_id=1, source_target_pairs={{0,1},{1,2},{2,3},{3,0},{4,5},{5,6},{6,7},{7,4},{8,9},{9,10},{10,1... | collective-permute-start | bytes 3145736 | tf_op jit(solution)/shard_map/ppermute | solution.py:227
  18.0 100.1 %collective-permute-start.20 = (bf16[2048,256]{1,0:T(8,128)(2,1)S(1)}, bf16[2048,256]{1,0:T(8,128)(2,1)S(1)}, u32[]{:S(2)}, u32[]{:S(2)}) collective-permute-start(bf16[2048,256]{1,0:T(8,128)(2,1)S(1)} %bitcast.37), channel_id=1, source_target_pairs={{0,3},{1,0},{2,1},{3,2},{4,7},{5,4},{6,5},{7,6},{8,11},{9,8},{10,9... | collective-permute-start | bytes 3145736 | tf_op jit(solution)/shard_map/ppermute | solution.py:227
  19.6 52.8 %collective-permute-start.1 = (bf16[256,256]{1,0:T(8,128)(2,1)S(1)}, bf16[256,256]{1,0:T(8,128)(2,1)S(1)}, u32[]{:S(2)}, u32[]{:S(2)}) collective-permute-start(bf16[256,256]{1,0:T(8,128)(2,1)S(1)} %get-tuple-element.9), channel_id=1, source_target_pairs={{0,64},{4,68},{8,72},{12,76},{16,80},{20,84},{24,88},{28,92},{32,9... | collective-permute-start | bytes 393224 | tf_op jit(solution)/shard_map/ppermute | solution.py:249
  22.0 58.5 %collective-permute-start.2 = (bf16[256,256]{1,0:T(8,128)(2,1)S(1)}, bf16[256,256]{1,0:T(8,128)(2,1)S(1)}, u32[]{:S(2)}, u32[]{:S(2)}) collective-permute-start(bf16[256,256]{1,0:T(8,128)(2,1)S(1)} %get-tuple-element.9), channel_id=1, source_target_pairs={{0,96},{4,100},{8,104},{12,108},{16,112},{20,116},{24,120},{28,124... | collective-permute-start | bytes 393224 | tf_op jit(solution)/shard_map/ppermute | solution.py:249
  66.6 16.9 %collective-permute-start.3 = (bf16[256,256]{1,0:T(8,128)(2,1)S(1)}, bf16[256,256]{1,0:T(8,128)(2,1)S(1)}, u32[]{:S(2)}, u32[]{:S(2)}) collective-permute-start(bf16[256,256]{1,0:T(8,128)(2,1)S(1)} %get-tuple-element.9), channel_id=1, source_target_pairs={{0,128},{4,132},{8,136},{12,140},{16,144},{20,148},{24,152},{28,15... | collective-permute-start | bytes 393224 | tf_op jit(solution)/shard_map/ppermute | solution.py:249
  72.5 41.9 %collective-permute-start.23 = (bf16[128,2048]{1,0:T(8,128)(2,1)S(1)}, bf16[128,2048]{1,0:T(8,128)(2,1)}, u32[]{:S(2)}, u32[]{:S(2)}) collective-permute-start(bf16[128,2048]{1,0:T(8,128)(2,1)S(1)} %get-tuple-element.5), channel_id=1, source_target_pairs={{0,1},{1,2},{2,3},{3,0},{4,5},{5,6},{6,7},{7,4},{8,9},{9,10},{10,1... | collective-permute-start | bytes 1572872 | tf_op jit(solution)/shard_map/ppermute | solution.py:227
  80.5 35.5 %collective-permute-start.25 = (bf16[128,2048]{1,0:T(8,128)(2,1)S(1)}, bf16[128,2048]{1,0:T(8,128)(2,1)}, u32[]{:S(2)}, u32[]{:S(2)}) collective-permute-start(bf16[128,2048]{1,0:T(8,128)(2,1)S(1)} %get-tuple-element.4), channel_id=1, source_target_pairs={{0,3},{1,0},{2,1},{3,2},{4,7},{5,4},{6,5},{7,6},{8,11},{9,8},{10,9... | collective-permute-start | bytes 1572872 | tf_op jit(solution)/shard_map/ppermute | solution.py:227
  83.5 13.2 %collective-permute-start.4 = (bf16[256,256]{1,0:T(8,128)(2,1)S(1)}, bf16[256,256]{1,0:T(8,128)(2,1)S(1)}, u32[]{:S(2)}, u32[]{:S(2)}) collective-permute-start(bf16[256,256]{1,0:T(8,128)(2,1)S(1)} %get-tuple-element.9), channel_id=1, source_target_pairs={{0,160},{4,164},{8,168},{12,172},{16,176},{20,180},{24,184},{28,18... | collective-permute-start | bytes 393224 | tf_op jit(solution)/shard_map/ppermute | solution.py:249
  96.6 8.7 %collective-permute-start.5 = (bf16[256,256]{1,0:T(8,128)(2,1)S(1)}, bf16[256,256]{1,0:T(8,128)(2,1)S(1)}, u32[]{:S(2)}, u32[]{:S(2)}) collective-permute-start(bf16[256,256]{1,0:T(8,128)(2,1)S(1)} %get-tuple-element.9), channel_id=1, source_target_pairs={{0,192},{4,196},{8,200},{12,204},{16,208},{20,212},{24,216},{28,22... | collective-permute-start | bytes 393224 | tf_op jit(solution)/shard_map/ppermute | solution.py:249
  105.4 6.9 %collective-permute-start.6 = (bf16[256,256]{1,0:T(8,128)(2,1)S(1)}, bf16[256,256]{1,0:T(8,128)(2,1)S(1)}, u32[]{:S(2)}, u32[]{:S(2)}) collective-permute-start(bf16[256,256]{1,0:T(8,128)(2,1)S(1)} %get-tuple-element.9), channel_id=1, source_target_pairs={{0,224},{4,228},{8,232},{12,236},{16,240},{20,244},{24,248},{28,25... | collective-permute-start | bytes 393224 | tf_op jit(solution)/shard_map/ppermute | solution.py:249
  112.3 16.3 %collective-permute-start.27 = (bf16[128,2048]{1,0:T(8,128)(2,1)S(1)}, bf16[128,2048]{1,0:T(8,128)(2,1)S(1)}, u32[]{:S(2)}, u32[]{:S(2)}) collective-permute-start(bf16[128,2048]{1,0:T(8,128)(2,1)S(1)} %get-tuple-element.4), channel_id=1, source_target_pairs={{0,1},{1,2},{2,3},{3,0},{4,5},{5,6},{6,7},{7,4},{8,9},{9,10},{10,1... | collective-permute-start | bytes 1572872 | tf_op jit(solution)/shard_map/ppermute | solution.py:227
  114.4 58.1 %collective-permute-start.18 = (bf16[2048,256]{1,0:T(8,128)(2,1)S(1)}, bf16[2048,256]{1,0:T(8,128)(2,1)S(1)}, u32[]{:S(2)}, u32[]{:S(2)}) collective-permute-start(bf16[2048,256]{1,0:T(8,128)(2,1)S(1)} %bitcast.38), channel_id=1, source_target_pairs={{0,1},{1,2},{2,3},{3,0},{4,5},{5,6},{6,7},{7,4},{8,9},{9,10},{10,1... | collective-permute-start | bytes 3145736 | tf_op jit(solution)/shard_map/ppermute | solution.py:227
  116.0 59.0 %collective-permute-start.19 = (bf16[2048,256]{1,0:T(8,128)(2,1)}, bf16[2048,256]{1,0:T(8,128)(2,1)S(1)}, u32[]{:S(2)}, u32[]{:S(2)}) collective-permute-start(bf16[2048,256]{1,0:T(8,128)(2,1)} %bitcast.8.refs_0_), channel_id=1, source_target_pairs={{0,3},{1,0},{2,1},{3,2},{4,7},{5,4},{6,5},{7,6},{8,11},{9,8},{10,9... | collective-permute-start | bytes 3145736 | tf_op jit(solution)/shard_map/ppermute | solution.py:227
  117.6 57.4 %copy-start.10 = (bf16[2048,256]{1,0:T(8,128)(2,1)}, bf16[2048,256]{1,0:T(8,128)(2,1)S(1)}, u32[]{:S(2)}) copy-start(bf16[2048,256]{1,0:T(8,128)(2,1)S(1)} %collective-permute-done.17.refs_2_) | copy-start | bytes 3145732
  117.6 57.4 %collective-permute-start.21 = (bf16[2048,256]{1,0:T(8,128)(2,1)S(1)}, bf16[2048,256]{1,0:T(8,128)(2,1)S(1)}, u32[]{:S(2)}, u32[]{:S(2)}) collective-permute-start(bf16[2048,256]{1,0:T(8,128)(2,1)S(1)} %collective-permute-done.17.refs_2_), channel_id=1, source_target_pairs={{0,1},{1,2},{2,3},{3,0},{4,5},{5,6},{6,7},{7,4},{8,9},{9,10},{10,1... | collective-permute-start | bytes 3145736 | tf_op jit(solution)/shard_map/ppermute | solution.py:227
  118.0 57.1 %copy-start.11 = (bf16[2048,256]{1,0:T(8,128)(2,1)}, bf16[2048,256]{1,0:T(8,128)(2,1)S(1)}, u32[]{:S(2)}) copy-start(bf16[2048,256]{1,0:T(8,128)(2,1)S(1)} %collective-permute-done.20.refs_5_) | copy-start | bytes 3145732
  118.0 58.4 %collective-permute-start.22 = (bf16[2048,256]{1,0:T(8,128)(2,1)S(1)}, bf16[2048,256]{1,0:T(8,128)(2,1)S(1)}, u32[]{:S(2)}, u32[]{:S(2)}) collective-permute-start(bf16[2048,256]{1,0:T(8,128)(2,1)S(1)} %collective-permute-done.20.refs_5_), channel_id=1, source_target_pairs={{0,3},{1,0},{2,1},{3,2},{4,7},{5,4},{6,5},{7,6},{8,11},{9,8},{10,9... | collective-permute-start | bytes 3145736 | tf_op jit(solution)/shard_map/ppermute | solution.py:227
  128.6 46.3 %copy-start.4 = (bf16[128,2048]{1,0:T(8,128)(2,1)}, bf16[128,2048]{1,0:T(8,128)(2,1)S(1)}, u32[]{:S(2)}) copy-start(bf16[128,2048]{1,0:T(8,128)(2,1)S(1)} %collective-permute-done.27.refs_2_) | copy-start | bytes 1572868
  128.6 43.5 %collective-permute-start.28 = (bf16[128,2048]{1,0:T(8,128)(2,1)S(1)}, bf16[128,2048]{1,0:T(8,128)(2,1)S(1)}, u32[]{:S(2)}, u32[]{:S(2)}) collective-permute-start(bf16[128,2048]{1,0:T(8,128)(2,1)S(1)} %get-tuple-element.5), channel_id=1, source_target_pairs={{0,3},{1,0},{2,1},{3,2},{4,7},{5,4},{6,5},{7,6},{8,11},{9,8},{10,9... | collective-permute-start | bytes 1572872 | tf_op jit(solution)/shard_map/ppermute | solution.py:227
  172.1 2.9 %copy-start.5 = (bf16[128,2048]{1,0:T(8,128)(2,1)}, bf16[128,2048]{1,0:T(8,128)(2,1)S(1)}, u32[]{:S(2)}) copy-start(bf16[128,2048]{1,0:T(8,128)(2,1)S(1)} %collective-permute-done.28.refs_3_) | copy-start | bytes 1572868
  172.1 40.5 %collective-permute-start.7 = (bf16[2048,256]{1,0:T(8,128)(2,1)S(1)}, bf16[2048,256]{1,0:T(8,128)(2,1)S(1)}, u32[]{:S(2)}, u32[]{:S(2)}) collective-permute-start(bf16[2048,256]{1,0:T(8,128)(2,1)S(1)} %constant_dynamic-update-slice_fusion.refs_0_), channel_id=1, source_target_pairs={{0,8},{4,12},{8,16},{12,20},{16,24},{20,28},{24,0},{28,4},{32,40},... | collective-permute-start | bytes 3145736 | tf_op jit(solution)/shard_map/ppermute | solution.py:249
  172.5 4.0 %copy-start.12 = (bf16[2048,256]{1,0:T(8,128)(2,1)}, bf16[2048,256]{1,0:T(8,128)(2,1)S(1)}, u32[]{:S(2)}) copy-start(bf16[2048,256]{1,0:T(8,128)(2,1)S(1)} %collective-permute-done.18.refs_3_) | copy-start | bytes 3145732
  172.5 40.4 %collective-permute-start.8 = (bf16[2048,256]{1,0:T(8,128)(2,1)S(1)}, bf16[2048,256]{1,0:T(8,128)(2,1)S(1)}, u32[]{:S(2)}, u32[]{:S(2)}) collective-permute-start(bf16[2048,256]{1,0:T(8,128)(2,1)S(1)} %constant_dynamic-update-slice_fusion.refs_0_), channel_id=1, source_target_pairs={{0,16},{4,20},{8,24},{12,28},{16,0},{20,4},{24,8},{28,12},{32,48},... | collective-permute-start | bytes 3145736 | tf_op jit(solution)/shard_map/ppermute | solution.py:249
  175.0 1.5 copy-start.13
  175.0 46.9 %collective-permute-start.9 = (bf16[2048,256]{1,0:T(8,128)(2,1)S(1)}, bf16[2048,256]{1,0:T(8,128)(2,1)}, u32[]{:S(2)}, u32[]{:S(2)}) collective-permute-start(bf16[2048,256]{1,0:T(8,128)(2,1)S(1)} %constant_dynamic-update-slice_fusion.refs_0_), channel_id=1, source_target_pairs={{0,24},{4,28},{8,0},{12,4},{16,8},{20,12},{24,16},{28,20},{32,56},... | collective-permute-start | bytes 3145736 | tf_op jit(solution)/shard_map/ppermute | solution.py:249
  175.1 1.4 copy-start.14
  175.1 21.1 %collective-permute-start.24 = (bf16[128,2048]{1,0:T(8,128)(2,1)}, bf16[128,2048]{1,0:T(8,128)(2,1)}, u32[]{:S(2)}, u32[]{:S(2)}) collective-permute-start(bf16[128,2048]{1,0:T(8,128)(2,1)} %collective-permute-done.23.refs_1_), channel_id=1, source_target_pairs={{0,1},{1,2},{2,3},{3,0},{4,5},{5,6},{6,7},{7,4},{8,9},{9,10},{10,1... | collective-permute-start | bytes 1572872 | tf_op jit(solution)/shard_map/ppermute | solution.py:227
  176.5 1.0 copy-start.15
  177.5 18.7 %collective-permute-start.26 = (bf16[128,2048]{1,0:T(8,128)(2,1)}, bf16[128,2048]{1,0:T(8,128)(2,1)}, u32[]{:S(2)}, u32[]{:S(2)}) collective-permute-start(bf16[128,2048]{1,0:T(8,128)(2,1)} %collective-permute-done.25.refs_4_), channel_id=1, source_target_pairs={{0,3},{1,0},{2,1},{3,2},{4,7},{5,4},{6,5},{7,6},{8,11},{9,8},{10,9... | collective-permute-start | bytes 1572872 | tf_op jit(solution)/shard_map/ppermute | solution.py:227
  201.4 20.5 %copy-start.6 = (bf16[256,2,128]{2,1,0:T(2,128)(2,1)S(1)}, bf16[256,2,128]{2,1,0:T(2,128)(2,1)}, u32[]{:S(2)}) copy-start(bf16[256,2,128]{2,1,0:T(2,128)(2,1)} %param.13) | copy-start | bytes 393220
  201.4 23.5 %copy-start.1 = (f32[2]{0:T(128)S(1)}, f32[2]{0:T(128)}, u32[]{:S(2)}) copy-start(f32[2]{0:T(128)} %lam_ref.1) | copy-start | bytes 28
  201.4 23.5 %copy-start.2 = (f32[128]{0:T(128)S(1)}, f32[128]{0:T(128)}, u32[]{:S(2)}) copy-start(f32[128]{0:T(128)} %param.17) | copy-start | bytes 1540
  201.4 70.8 %all-to-all-start.1 = ((bf16[64,8,2048]{2,1,0:T(8,128)(2,1)}), bf16[64,8,2048]{2,1,0:T(8,128)(2,1)}, u32[]{:S(2)}, u32[]{:S(2)}) async-start(bf16[64,8,2048]{2,1,0:T(8,128)(2,1)} %bitcast.31), calls=%async_computation.1 | async-start | bytes 4194304 | tf_op jit(solution)/shard_map/all_to_all | solution.py:282
  212.3 10.3 %collective-permute-start.10 = (bf16[2048,256]{1,0:T(8,128)(2,1)S(1)}, bf16[2048,256]{1,0:T(8,128)(2,1)}, u32[]{:S(2)}, u32[]{:S(2)}) collective-permute-start(bf16[2048,256]{1,0:T(8,128)(2,1)S(1)} %constant_dynamic-update-slice_fusion.refs_0_), channel_id=1, source_target_pairs={{0,4},{4,0},{8,12},{12,8},{16,20},{20,16},{24,28},{28,24},{32,36},... | collective-permute-start | bytes 3145736 | tf_op jit(solution)/shard_map/ppermute | solution.py:249
  212.5 10.1 %collective-permute-start.11 = (bf16[2048,256]{1,0:T(8,128)(2,1)S(1)}, bf16[2048,256]{1,0:T(8,128)(2,1)}, u32[]{:S(2)}, u32[]{:S(2)}) collective-permute-start(bf16[2048,256]{1,0:T(8,128)(2,1)S(1)} %collective-permute-done.7.refs_1_), channel_id=1, source_target_pairs={{0,4},{4,0},{8,12},{12,8},{16,20},{20,16},{24,28},{28,24},{32,36},... | collective-permute-start | bytes 3145736 | tf_op jit(solution)/shard_map/ppermute | solution.py:249
  212.9 9.7 %collective-permute-start.12 = (bf16[2048,256]{1,0:T(8,128)(2,1)S(1)}, bf16[2048,256]{1,0:T(8,128)(2,1)}, u32[]{:S(2)}, u32[]{:S(2)}) collective-permute-start(bf16[2048,256]{1,0:T(8,128)(2,1)S(1)} %collective-permute-done.8.refs_2_), channel_id=1, source_target_pairs={{0,4},{4,0},{8,12},{12,8},{16,20},{20,16},{24,28},{28,24},{32,36},... | collective-permute-start | bytes 3145736 | tf_op jit(solution)/shard_map/ppermute | solution.py:249
  221.9 3.0 %collective-permute-start.13 = (bf16[2048,256]{1,0:T(8,128)(2,1)}, bf16[2048,256]{1,0:T(8,128)(2,1)}, u32[]{:S(2)}, u32[]{:S(2)}) collective-permute-start(bf16[2048,256]{1,0:T(8,128)(2,1)} %collective-permute-done.9.refs_3_), channel_id=1, source_target_pairs={{0,4},{4,0},{8,12},{12,8},{16,20},{20,16},{24,28},{28,24},{32,36},... | collective-permute-start | bytes 3145736 | tf_op jit(solution)/shard_map/ppermute | solution.py:249
  257.6 7.4 %collective-permute-start.15 = (bf16[64,256]{1,0:T(8,128)(2,1)S(1)}, bf16[64,256]{1,0:T(8,128)(2,1)S(1)}, u32[]{:S(2)}, u32[]{:S(2)}) collective-permute-start(bf16[64,256]{1,0:T(8,128)(2,1)S(1)} %get-tuple-element.8), channel_id=1, source_target_pairs={{0,2},{1,3},{2,0},{3,1},{4,6},{5,7},{6,4},{7,5},{8,10},{9,11},{10,... | collective-permute-start | bytes 98312 | tf_op jit(solution)/shard_map/ppermute | solution.py:227
  261.7 5.1 %collective-permute-start.14 = (bf16[64,256]{1,0:T(8,128)(2,1)S(1)}, bf16[64,256]{1,0:T(8,128)(2,1)S(1)}, u32[]{:S(2)}, u32[]{:S(2)}) collective-permute-start(bf16[64,256]{1,0:T(8,128)(2,1)S(1)} %get-tuple-element.6), channel_id=1, source_target_pairs={{0,1},{1,2},{2,3},{3,0},{4,5},{5,6},{6,7},{7,4},{8,9},{9,10},{10,1... | collective-permute-start | bytes 98312 | tf_op jit(solution)/shard_map/ppermute | solution.py:227
  263.6 4.8 %collective-permute-start.16 = (bf16[64,256]{1,0:T(8,128)(2,1)S(1)}, bf16[64,256]{1,0:T(8,128)(2,1)S(1)}, u32[]{:S(2)}, u32[]{:S(2)}) collective-permute-start(bf16[64,256]{1,0:T(8,128)(2,1)S(1)} %get-tuple-element.7), channel_id=1, source_target_pairs={{0,3},{1,0},{2,1},{3,2},{4,7},{5,4},{6,5},{7,6},{8,11},{9,8},{10,9... | collective-permute-start | bytes 98312 | tf_op jit(solution)/shard_map/ppermute | solution.py:227
